TPU v7x, 256 devices: a whole 4x4x8 slice. The times are simulated.
256 devices in a mesh: ep: 128 (over z, y, x), tp: 2 (over core).
Axes of the slice: x: 4, y: 4, z: 8, core: 2. Of those that a mesh axis runs over, the one named last changes fastest.
Arguments:
- tokens_in: bfloat16 [4096, 2048], P('ep'), may hold values from -6 to 6
- state_in: float32 [4096, 8, 64, 64], P('ep', 'tp'), may hold values from -4 to 4
- norm_mix: bfloat16 [2048], replicated, may hold values from 0.099609375 to 1.8984375
- w_recept: bfloat16 [2048, 512], P(None, 'tp'), may hold values from -0.125 to 0.125
- w_key: bfloat16 [2048, 512], P(None, 'tp'), may hold values from -0.125 to 0.125
- w_value: bfloat16 [2048, 512], P(None, 'tp'), may hold values from -0.125 to 0.125
- decay_down: bfloat16 [2048, 64], replicated, may hold values from -0.125 to 0.125
- decay_up: bfloat16 [64, 512], P(None, 'tp'), may hold values from -0.75 to 0.75
- decay_base: float32 [512], P('tp'), may hold values from -4 to 2
- iclr_down: bfloat16 [2048, 64], replicated, may hold values from -0.125 to 0.125
- iclr_up: bfloat16 [64, 512], P(None, 'tp'), may hold values from -0.75 to 0.75
- iclr_base: float32 [512], P('tp'), may hold values from -4 to 4
- key_scale: bfloat16 [512], P('tp'), may hold values from 0.099609375 to 1.8984375
- key_mix: bfloat16 [512], P('tp'), may hold values from 0.099609375 to 1.8984375
- w_out: bfloat16 [512, 2048], P('tp'), may hold values from -0.046875 to 0.046875
- norm_moe: bfloat16 [2048], replicated, may hold values from 0.099609375 to 1.8984375
- router_group: bfloat16 [2048, 16], replicated, may hold values from -0.125 to 0.125
- router_expert: bfloat16 [2048, 128], replicated, may hold values from -0.125 to 0.125
- routes: int32 [4096, 4], P('ep'), may hold values from 0 to 127, as said below
- expert_gate: bfloat16 [128, 2048, 256], P('ep', None, 'tp'), may hold values from -0.125 to 0.125
- expert_up: bfloat16 [128, 2048, 256], P('ep', None, 'tp'), may hold values from -0.125 to 0.125
- expert_down: bfloat16 [128, 256, 2048], P('ep', 'tp'), may hold values from -1.5 to 1.5
Outputs:
- layer_out: bfloat16 [4096, 2048], P('ep', 'tp')
- state_out: float32 [4096, 8, 64, 64], P('ep', 'tp')
Inputs may be any that keep to these rules, and one draw needn't show every extreme that they name: `routes`: each row names 4 different experts of one group (the same value of id // 8). Among the rows of one device no expert is named by more than 2 rows, and in every draw one expert is named by exactly 2 rows of every device.
All inputs are finite; a program needn't handle non-finite values.
Results may differ from a plain program's by a relative error of at most 0.018.
Values may be sent and summed in bfloat16 or wider, within the bound.
A program may use at most 64 MiB of HBM per device.

v0:
```python
import jax
import jax.numpy as jnp
from jax import lax
from jax.sharding import PartitionSpec as P


def total_of_pieces(value, axis):
    tiles = lax.all_gather(value, axis)
    return tiles.sum(axis=0)


def copy_for_each(value, axis):
    copies = jnp.broadcast_to(value, (lax.axis_size(axis), *value.shape))
    return lax.all_to_all(copies, axis, split_axis=0, concat_axis=0, tiled=True)


def joined_along(tiles, dim):
    tiles = jnp.moveaxis(tiles, 0, dim)
    shape = tiles.shape
    return tiles.reshape(*shape[:dim], shape[dim] * shape[dim + 1], *shape[dim + 2 :])


def gather_directly(value, axis, dim):
    tiles = copy_for_each(value, axis)
    return joined_along(tiles, dim)


def split_up(value, dim, size):
    before, after = (value.shape[:dim], value.shape[dim + 1 :])
    return jnp.moveaxis(value.reshape(*before, size, -1, *after), dim, 0)


def sum_at_owner(value, axis, dim):
    size = lax.axis_size(axis)
    tiles = lax.all_to_all(split_up(value, dim, size), axis, 0, 0, tiled=True)
    return jnp.sum(tiles.astype(jnp.float32), axis=0)


def rms_scale(values, weights):
    values32 = values.astype(jnp.float32)
    factor = lax.rsqrt(jnp.mean(values32 * values32, axis=-1, keepdims=True) + 1e-06)
    return (values32 * factor * weights.astype(jnp.float32)).astype(jnp.bfloat16)


def shards(
    tokens_in,
    state_in,
    norm_mix,
    w_recept,
    w_key,
    w_value,
    decay_down,
    decay_up,
    decay_base,
    iclr_down,
    iclr_up,
    iclr_base,
    key_scale,
    key_mix,
    w_out,
    norm_moe,
    router_group,
    router_expert,
    routes,
    expert_gate,
    expert_up,
    expert_down,
):
    f32 = jnp.float32
    bf16 = jnp.bfloat16
    seq_count = tokens_in.shape[0]
    width_model = tokens_in.shape[1]
    heads_here = state_in.shape[1]
    head_size = state_in.shape[-1]
    tp_count = lax.axis_size("tp")
    ep_count = lax.axis_size("ep")
    half_width = width_model // tp_count

    def split_heads(values):
        return values.astype(f32).reshape(values.shape[0], heads_here, head_size)

    normed = rms_scale(tokens_in, norm_mix)
    recept = jnp.dot(normed, w_recept, preferred_element_type=f32).astype(bf16)
    key_rows = jnp.dot(normed, w_key, preferred_element_type=f32).astype(bf16)
    value_rows = jnp.dot(normed, w_value, preferred_element_type=f32).astype(bf16)
    decay_low = jnp.tanh(jnp.dot(normed, decay_down, preferred_element_type=f32)).astype(bf16)
    iclr_low = jnp.dot(normed, iclr_down, preferred_element_type=f32).astype(bf16)
    log_rate = (
        -jax.nn.softplus(-(decay_base + jnp.dot(decay_low, decay_up, preferred_element_type=f32)))
        - 0.5
    )
    decays = jnp.exp(-jnp.exp(log_rate))
    learn_rate = jax.nn.sigmoid(iclr_base + jnp.dot(iclr_low, iclr_up, preferred_element_type=f32))
    recept_heads = split_heads(recept)
    key_heads = split_heads(key_rows)
    value_heads = split_heads(value_rows)
    rate_heads = split_heads(learn_rate)
    decay_heads = split_heads(decays)
    scaled = key_heads * key_scale.astype(f32).reshape(heads_here, head_size)
    unit_key = scaled * lax.rsqrt(jnp.sum(scaled * scaled, axis=-1, keepdims=True) + 1e-06)
    key_mod = key_heads * (
        1.0 + (rate_heads - 1.0) * key_mix.astype(f32).reshape(heads_here, head_size)
    )
    removed = jnp.einsum("shvk,shk->shv", state_in, unit_key)
    state_out = (
        state_in * decay_heads[:, :, None, :]
        - removed[..., None] * (unit_key * rate_heads)[:, :, None, :]
        + value_heads[..., None] * key_mod[:, :, None, :]
    )
    mixed = (
        jnp.einsum("shvk,shk->shv", state_out, recept_heads)
        .reshape(seq_count, heads_here * head_size)
        .astype(bf16)
    )
    partial_value = jnp.dot(mixed, w_out, preferred_element_type=f32)
    mixer_out = total_of_pieces(partial_value, "tp").astype(bf16)
    x_mid = (tokens_in.astype(f32) + mixer_out.astype(f32)).astype(bf16)
    own_half = lax.dynamic_slice_in_dim(x_mid, lax.axis_index("tp") * half_width, half_width, 1)
    moe_in = rms_scale(x_mid, norm_moe)
    n_groups = router_group.shape[1]
    experts_all = router_expert.shape[1]
    group_size = experts_all // n_groups
    top_count = routes.shape[1]
    group_id = routes[:, 0] // group_size
    group_logit = jnp.dot(moe_in, router_group, preferred_element_type=f32)
    group_hit = group_id[:, None] == jnp.arange(n_groups)[None, :]
    group_prob = jax.nn.sigmoid(jnp.sum(jnp.where(group_hit, group_logit, 0.0), axis=1))
    expert_logit = jnp.dot(moe_in, router_expert, preferred_element_type=f32)
    expert_hit = routes[:, :, None] == jnp.arange(experts_all)[None, None, :]
    scores = jax.nn.sigmoid(jnp.sum(jnp.where(expert_hit, expert_logit[:, None, :], 0.0), axis=2))
    route_weight = group_prob[:, None] * scores / jnp.sum(scores, axis=1, keepdims=True)
    capacity = max(2, 2 * seq_count * top_count // ep_count)
    flat_routes = routes.reshape(-1)
    slot_count = flat_routes.shape[0]
    matches = flat_routes[:, None] == flat_routes[None, :]
    earlier = jnp.arange(slot_count)[:, None] < jnp.arange(slot_count)[None, :]
    position = jnp.sum(jnp.logical_and(matches, earlier).astype(jnp.int32), axis=0)
    target = flat_routes * capacity + position
    buffer_rows = experts_all * capacity
    placement = jnp.sum(
        (
            target.reshape(seq_count, top_count)[:, :, None]
            == jnp.arange(buffer_rows)[None, None, :]
        ).astype(bf16),
        axis=1,
    )
    source = lax.dynamic_slice_in_dim(moe_in, lax.axis_index("tp") * half_width, half_width, 1)
    outgoing = jnp.einsum("se,sd->ed", placement, source, preferred_element_type=f32).astype(bf16)
    outgoing = outgoing.reshape(experts_all, capacity, source.shape[1])
    complete = gather_directly(
        lax.all_to_all(outgoing, "ep", split_axis=0, concat_axis=0, tiled=True), "tp", 2
    )
    flat_rows = complete.reshape(-1, width_model)
    gate_part = jnp.dot(flat_rows, expert_gate[0], preferred_element_type=f32)
    up_part = jnp.dot(flat_rows, expert_up[0], preferred_element_type=f32)
    hidden = (jax.nn.silu(gate_part) * up_part).astype(bf16)
    partial_out = jnp.dot(hidden, expert_down[0], preferred_element_type=f32)
    partial_out = partial_out.reshape(complete.shape[0], complete.shape[1], width_model)
    result = sum_at_owner(partial_out.astype(jnp.bfloat16), "tp", 2).astype(bf16)
    returned = lax.all_to_all(result, "ep", split_axis=0, concat_axis=0, tiled=True)
    flat_back = returned.reshape(buffer_rows, half_width)
    chooser = (target[:, None] == jnp.arange(buffer_rows)[None, :]).astype(bf16)
    gathered = jnp.dot(chooser, flat_back, preferred_element_type=f32).reshape(
        seq_count, top_count, half_width
    )
    moe_out = jnp.sum(route_weight[:, :, None] * gathered, axis=1)
    layer_out = (own_half.astype(f32) + moe_out).astype(bf16)
    return (layer_out, state_out)


def solution(mesh):
    in_specs = (
        P("ep", None),
        P("ep", "tp", None, None),
        P(),
        P(None, "tp"),
        P(None, "tp"),
        P(None, "tp"),
        P(),
        P(None, "tp"),
        P("tp"),
        P(),
        P(None, "tp"),
        P("tp"),
        P("tp"),
        P("tp"),
        P("tp", None),
        P(),
        P(),
        P(),
        P("ep", None),
        P("ep", None, "tp"),
        P("ep", None, "tp"),
        P("ep", "tp", None),
    )
    out_specs = (P("ep", "tp"), P("ep", "tp", None, None))
    return jax.shard_map(shards, mesh=mesh, in_specs=in_specs, out_specs=out_specs, check_vma=False)
```

profile of v0, /device:TPU:1, one launch (start us, length us, event | category | flops | bytes accessed | tf_op | source)
XLA Modules:
  0.0 106.1 jit_solution(7048661815597873810)
XLA Ops:
  0.7 1.1 %fusion.18 = f32[32]{0:T(128)S(1)} fusion(bf16[32,2048]{1,0:T(8,128)(2,1)} %param.22), kind=kLoop, calls=%fused_computation.37 | loop fusion | flops 196576 | bytes 131200 | tf_op jit(solution)/shard_map/reduce_sum | solution.py:41
  1.8 0.7 reshape.178
  2.6 0.7 reshape.180
  3.3 0.7 convert_element_type.81
  4.0 0.7 convert_element_type.95
  4.7 0.8 copy.66
  5.9 0.7 multiply_add_fusion.1
  6.7 1.6 %convolution_convert_fusion.2 = bf16[32,256]{1,0:T(8,128)(2,1)S(1)} fusion(bf16[2048,256]{1,0:T(8,128)(2,1)} %param.25, bf16[32,2048]{1,0:T(8,128)(2,1)} %param.22, f32[2048]{0:T(1024)S(1)} %convert_element_type.81, f32[32]{0:T(128)S(1)} %add_rsqrt_fusion.2), kind=kOutput, calls=%fused_computation.14 | convolution fusion | flops 33824768 | bytes 1204352 | tf_op jit(solution)/shard_map/dot_general | solution.py:83
  8.3 1.6 %fusion.8 = f32[32,256]{1,0:T(8,128)S(1)} fusion(bf16[2048,256]{1,0:T(8,128)(2,1)} %param.26, bf16[32,2048]{1,0:T(8,128)(2,1)} %param.22, f32[2048]{0:T(1024)S(1)} %convert_element_type.81, f32[32]{0:T(128)S(1)} %add_rsqrt_fusion.2), kind=kOutput, calls=%fused_computation.18 | convolution fusion | flops 33832960 | bytes 1220736 | tf_op jit(solution)/shard_map/dot_general | solution.py:84
  10.1 1.4 %fusion.5 = f32[32,256]{1,0:T(8,128)S(1)} fusion(bf16[64,256]{1,0:T(8,128)(2,1)} %param.32, bf16[2048,64]{0,1:T(8,128)(2,1)} %param.31, f32[256]{0:T(256)} %param.33, bf16[32,2048]{1,0:T(8,128)(2,1)} %param.22, f32[2048]{0:T(1024)S(1)} %convert_element_type.81, f32[32]{0:T(128)S(1)} %add_rsqrt_fusion.2), kind=kOutput, calls=%fused_computation.11 | convolution fusion | flops 9734144 | bytes 468096 | tf_op jit(solution)/shard_map/dot_general | solution.py:93
  11.6 1.6 %fusion.7 = f32[32,256]{1,0:T(8,128)S(1)} fusion(bf16[2048,256]{1,0:T(8,128)(2,1)} %param.27, bf16[32,2048]{1,0:T(8,128)(2,1)} %param.22, f32[2048]{0:T(1024)S(1)} %convert_element_type.81, f32[32]{0:T(128)S(1)} %add_rsqrt_fusion.2), kind=kOutput, calls=%fused_computation.16 | convolution fusion | flops 33832960 | bytes 1220736 | tf_op jit(solution)/shard_map/dot_general | solution.py:85
  14.2 3.5 %fusion.47 = f32[32,4,1,64]{3,2,1,0:T(1,128)S(1)} fusion(f32[32,4,64,1]{2,3,1,0:T(1,128)S(1)} %bitcast.65, f32[32,4,64,64]{3,2,1,0:T(8,128)} %param.23), kind=kOutput, calls=%fused_computation.80 | convolution fusion | flops 1048576 | bytes 2162688 | tf_op jit(solution)/shard_map/shvk,shk->shv/dot_general | solution.py:104
  17.7 2.7 %multiply_add_fusion = f32[32,4,64,64]{3,2,1,0:T(8,128)S(1)} fusion(f32[32,4,64,64]{3,2,1,0:T(8,128)S(1)} %copy-done.1, f32[32,4,64]{2,1,0:T(4,128)S(1)} %get-tuple-element.6, f32[32,4,64]{2,1,0:T(4,128)S(1)} %reshape.179, f32[32,4,64]{2,1,0:T(4,128)S(1)} %get-tuple-element.4, f32[32,4,64]{2,1,0:T(4,128)S(1)} %bitcast.63, f32[32,4,64]{2,1,0:T(4,128)S(1)} %mul.190), kind=kLoop, calls=%fused_computation | loop fusion | flops 2621440 | bytes 4358144 | tf_op jit(solution)/shard_map/add | solution.py:106
  20.4 2.0 %copy-done.2 = f32[32,4,64,64]{3,2,1,0:T(8,128)} copy-done((f32[32,4,64,64]{3,2,1,0:T(8,128)}, f32[32,4,64,64]{3,2,1,0:T(8,128)S(1)}, u32[]{:S(2)}) %copy-start.2) | copy-done | bytes 2097176
  22.4 1.2 %fusion.48 = f32[32,4,1,64]{3,2,1,0:T(1,128)S(1)} fusion(f32[32,4,64,64]{3,2,1,0:T(8,128)S(1)} %multiply_add_fusion, bf16[32,4,64,1]{2,3,1,0:T(2,128)(2,1)S(1)} %reshape.189), kind=kOutput, calls=%fused_computation.81 | convolution fusion | flops 1048576 | bytes 2146304 | tf_op jit(solution)/shard_map/shvk,shk->shv/dot_general | solution.py:111
  24.0 5.0 %all-gather = f32[64,2048]{1,0:T(8,128)S(1)} all-gather(f32[32,2048]{1,0:T(8,128)S(1)} %fusion.49), channel_id=2, replica_groups=mesh['ep'=128,'tp'=2] {'tp'}, dimensions={0}, use_global_device_ids=true | all-gather | bytes 786432 | tf_op jit(solution)/shard_map/all_gather | solution.py:8
  29.9 32.4 %all_to_all.20 = bf16[128,2,1024]{2,1,0:T(2,128)(2,1)S(1)} all-to-all(bf16[128,2,1024]{2,1,0:T(2,128)(2,1)S(1)} %reshape.173), channel_id=1, replica_groups=mesh['ep'=128,'tp'=2] {'ep'}, dimensions={0} | all-to-all | bytes 1048576 | tf_op jit(solution)/shard_map/all_to_all | solution.py:151
  62.9 7.1 %all_to_all.21 = bf16[2,128,2,1024]{3,2,1,0:T(2,128)(2,1)S(1)} all-to-all(bf16[2,128,2,1024]{3,2,1,0:T(2,128)(2,1)S(1)} %broadcast_in_dim.17), channel_id=1, replica_groups=mesh['ep'=128,'tp'=2] {'tp'}, dimensions={0} | all-to-all | bytes 2097152 | tf_op jit(solution)/shard_map/all_to_all | solution.py:14
  70.0 1.6 %copy.68 = bf16[128,2,2,1024]{3,2,1,0:T(2,128)(2,1)S(1)} copy(bf16[128,2,2,1024]{3,1,0,2:T(2,128)(2,1)S(1)} %bitcast.56) | data formatting | bytes 2097152 | tf_op jit(solution)/shard_map/transpose | solution.py:18
  73.4 4.7 %all_to_all.22 = bf16[2,128,2,1024]{3,1,2,0:T(8,128)(2,1)S(1)} all-to-all(bf16[2,128,2,1024]{3,1,2,0:T(8,128)(2,1)S(1)} %bitcast.59), channel_id=1, replica_groups=mesh['ep'=128,'tp'=2] {'tp'}, dimensions={0} | all-to-all | bytes 2097152 | tf_op jit(solution)/shard_map/all_to_all | solution.py:35
  78.3 1.3 %copy.72 = bf16[128,2,1024]{2,1,0:T(2,128)(2,1)} copy(bf16[128,2,1024]{2,0,1:T(8,128)(2,1)S(1)} %reduce_sum.117) | data formatting | bytes 1048576 | tf_op jit(solution)/shard_map/reduce_sum | solution.py:36
  79.7 6.2 %all-to-all-start.3 = ((bf16[128,2,1024]{2,1,0:T(2,128)(2,1)}), bf16[128,2,1024]{2,1,0:T(2,128)(2,1)S(1)}, u32[]{:S(2)}, u32[]{:S(2)}) async-start(bf16[128,2,1024]{2,1,0:T(2,128)(2,1)} %copy.72), calls=%async_computation.3 | async-start | bytes 1048576 | tf_op jit(solution)/shard_map/all_to_all | solution.py:160
  86.5 18.5 %all-to-all-done.3 = bf16[128,2,1024]{2,1,0:T(2,128)(2,1)S(1)} async-done(((bf16[128,2,1024]{2,1,0:T(2,128)(2,1)}), bf16[128,2,1024]{2,1,0:T(2,128)(2,1)S(1)}, u32[]{:S(2)}, u32[]{:S(2)}) %all-to-all-start.3) | async-done | bytes 524320 | tf_op jit(solution)/shard_map/all_to_all | solution.py:160
  105.5 0.7 add_convert_fusion
  (65 shorter events, 6.4 us)
Async XLA Ops:
  0.6 23.1 %copy-start = (bf16[256,2048]{1,0:T(8,128)(2,1)S(1)}, bf16[256,2048]{1,0:T(8,128)(2,1)}, u32[]{:S(2)}) copy-start(bf16[256,2048]{1,0:T(8,128)(2,1)} %param.36) | copy-start | bytes 3145732
  0.6 12.6 %copy-start.3 = (bf16[32,2048]{1,0:T(8,128)(2,1)S(1)}, bf16[32,2048]{1,0:T(8,128)(2,1)}, u32[]{:S(2)}) copy-start(bf16[32,2048]{1,0:T(8,128)(2,1)} %param.22) | copy-start | bytes 393220
  0.7 12.6 %copy-start.12 = (f32[256]{0:T(256)S(1)}, f32[256]{0:T(256)}, u32[]{:S(2)}) copy-start(f32[256]{0:T(256)} %param.30) | copy-start | bytes 3076
  0.7 12.6 %copy-start.11 = (bf16[64,256]{1,0:T(8,128)(2,1)S(1)}, bf16[64,256]{1,0:T(8,128)(2,1)}, u32[]{:S(2)}) copy-start(bf16[64,256]{1,0:T(8,128)(2,1)} %param.29) | copy-start | bytes 98308
  0.7 12.6 %copy-start.10 = (bf16[2048,64]{0,1:T(8,128)(2,1)S(1)}, bf16[2048,64]{0,1:T(8,128)(2,1)}, u32[]{:S(2)}) copy-start(bf16[2048,64]{0,1:T(8,128)(2,1)} %param.28) | copy-start | bytes 786436
  14.0 3.6 %copy-start.1 = (f32[32,4,64,64]{3,2,1,0:T(8,128)S(1)}, f32[32,4,64,64]{3,2,1,0:T(8,128)}, u32[]{:S(2)}) copy-start(f32[32,4,64,64]{3,2,1,0:T(8,128)} %param.23) | copy-start | bytes 6291460
  20.4 2.0 %copy-start.2 = (f32[32,4,64,64]{3,2,1,0:T(8,128)}, f32[32,4,64,64]{3,2,1,0:T(8,128)S(1)}, u32[]{:S(2)}) copy-start(f32[32,4,64,64]{3,2,1,0:T(8,128)S(1)} %multiply_add_fusion) | copy-start | bytes 6291460
  62.3 9.6 %copy-start.5 = (bf16[1,2048,128]{2,1,0:T(8,128)(2,1)S(1)}, bf16[1,2048,128]{2,1,0:T(8,128)(2,1)}, u32[]{:S(2)}) copy-start(bf16[1,2048,128]{2,1,0:T(8,128)(2,1)} %param.41) | copy-start | bytes 1572868
  62.9 9.5 %copy-start.9 = (bf16[1,2048,128]{2,1,0:T(8,128)(2,1)S(1)}, bf16[1,2048,128]{2,1,0:T(8,128)(2,1)}, u32[]{:S(2)}) copy-start(bf16[1,2048,128]{2,1,0:T(8,128)(2,1)} %param.42) | copy-start | bytes 1572868
  70.0 2.8 %copy-start.4 = (bf16[1,128,2048]{2,1,0:T(8,128)(2,1)S(1)}, bf16[1,128,2048]{2,1,0:T(8,128)(2,1)}, u32[]{:S(2)}) copy-start(bf16[1,128,2048]{2,1,0:T(8,128)(2,1)} %param.43) | copy-start | bytes 1572868
  73.2 12.6 %copy-start.6 = (bf16[2048,128]{1,0:T(8,128)(2,1)S(1)}, bf16[2048,128]{1,0:T(8,128)(2,1)}, u32[]{:S(2)}) copy-start(bf16[2048,128]{1,0:T(8,128)(2,1)} %param.39) | copy-start | bytes 1572868
  73.2 12.8 %copy-start.8 = (s32[32,4]{0,1:T(4,128)S(1)}, s32[32,4]{0,1:T(4,128)}, u32[]{:S(2)}) copy-start(s32[32,4]{0,1:T(4,128)} %param.40) | copy-start | bytes 1540
  73.3 13.0 %copy-start.7 = (bf16[2048,16]{0,1:T(8,128)(2,1)S(1)}, bf16[2048,16]{0,1:T(8,128)(2,1)}, u32[]{:S(2)}) copy-start(bf16[2048,16]{0,1:T(8,128)(2,1)} %param.38) | copy-start | bytes 196612
  79.7 25.4 %all-to-all-start.3 = ((bf16[128,2,1024]{2,1,0:T(2,128)(2,1)}), bf16[128,2,1024]{2,1,0:T(2,128)(2,1)S(1)}, u32[]{:S(2)}, u32[]{:S(2)}) async-start(bf16[128,2,1024]{2,1,0:T(2,128)(2,1)} %copy.72), calls=%async_computation.3 | async-start | bytes 1048576 | tf_op jit(solution)/shard_map/all_to_all | solution.py:160
where the time goes:
time: 107 us; the launch traced here: 106 us
  blocking collectives  49.3 us (46%)
  waiting for transfers between devices  18.5 us (17%)
  matrix products  13.9 us (13%)
  local copies, waits for them, and re-layouts  9.4 us (9%)
  other arithmetic  7.83 us (7%)
  starting transfers between devices  6.17 us (6%)
    all_to_all x1, blocking collectives, shards(): lax.all_to_all(outgoing, 'ep', split_axis=0, concat_axis=0, tiled=True)  32.4 us
    all_to_all x1, waiting for transfers between devices, shards(): lax.all_to_all(result, 'ep', split_axis=0, concat_axis=0, tiled=True)  18.5 us
    all_to_all x1, blocking collectives, copy_for_each(): return lax.all_to_all(copies, axis, split_axis=0, concat_axis=0, tiled=True)  7.13 us
    all_to_all x1, starting transfers between devices, shards(): lax.all_to_all(result, 'ep', split_axis=0, concat_axis=0, tiled=True)  6.17 us
    all_gather x1, blocking collectives, total_of_pieces(): tiles = lax.all_gather(value, axis)  5.02 us
    all_to_all x1, blocking collectives, sum_at_owner(): tiles = lax.all_to_all(split_up(value, dim, size), axis, 0, 0, tiled=True)  4.71 us
    dot_general x1, matrix products, shards(): removed = jnp.einsum('shvk,shk->shv', state_in, unit_key)  3.51 us
    unnamed x28, local copies, waits for them, and re-layouts  3.1 us
  transfers between devices with their start and end apart: 1, of which 1 were waited for; matrix products, arithmetic and copies ran while one was open for 1% of the time, Pallas kernels for 0%

commit v1 on v0

v1 whole, which is shorter than its diff:
```python
import jax
import jax.numpy as jnp
from jax import lax
from jax.experimental import pallas as pl
from jax.experimental.pallas import tpu as pltpu
from jax.sharding import PartitionSpec as P

MESH = pl.DeviceIdType.MESH
F32 = jnp.float32
BF16 = jnp.bfloat16
NZ, NY, NX = 8, 4, 4
NQ = NY * NX


def rms_scale(values, weights):
    values32 = values.astype(jnp.float32)
    factor = lax.rsqrt(jnp.mean(values32 * values32, axis=-1, keepdims=True) + 1e-06)
    return (values32 * factor * weights.astype(jnp.float32)).astype(jnp.bfloat16)


def iota(shape, dim):
    return lax.broadcasted_iota(jnp.int32, shape, dim)


def nt_dot(a, b):
    return lax.dot_general(a, b, (((1,), (1,)), ((), ())), preferred_element_type=F32)


def exchange_kernel(
    p1_ref, p1t_ref, meta_ref, src_ref, own_ref, gate_ref, up_ref, down_ref,
    out_ref,
    wg, wu, wd, send1, recv1, recvm, send2, recv2, part, partr, res, ret, comb, back,
    wsem, w_ss, w_rs, s1s, s1r, sms, smr, s2s, s2r, ps, pr, s3s, s3r, s4s, s4r,
):
    half = src_ref.shape[1]
    fh = gate_ref.shape[2]
    e = lax.axis_index("ep")
    t = lax.axis_index("tp")
    z, y, x = e // NQ, lax.rem(e // NX, NY), lax.rem(e, NX)
    me_q = lax.rem(e, NQ)
    partner = (e, 1 - t)

    def z_peer(d):
        return lax.rem(z + d + NZ, NZ) * NQ + me_q

    def q_of(a, b):
        return lax.rem(y + a + NY, NY) * NX + lax.rem(x + b + NX, NX)

    plane = [(a, b) for a in range(NY) for b in range(NX) if a or b]

    barrier = pltpu.get_barrier_semaphore()
    pl.semaphore_signal(barrier, inc=1, device_id=partner, device_id_type=MESH)
    for d in range(1, NZ):
        pl.semaphore_signal(barrier, inc=1, device_id=(z_peer(d), t), device_id_type=MESH)
    for a, b in plane:
        pl.semaphore_signal(barrier, inc=1, device_id=(z * NQ + q_of(a, b), t), device_id_type=MESH)

    mine = pl.ds(pl.multiple_of(t * half, half), half)
    theirs = pl.ds(pl.multiple_of((1 - t) * half, half), half)
    lanes = pl.ds(pl.multiple_of(t * fh, fh), fh)
    local = [
        pltpu.make_async_copy(gate_ref.at[0, mine], wg.at[:, lanes], wsem.at[0]),
        pltpu.make_async_copy(up_ref.at[0, mine], wu.at[:, lanes], wsem.at[1]),
        pltpu.make_async_copy(down_ref.at[0, :, mine], wd.at[lanes], wsem.at[2]),
    ]
    for copy in local:
        copy.start()

    rows = jnp.dot(p1_ref[...], src_ref[...], preferred_element_type=F32)
    for i in range(NZ):
        send1[i] = rows[8 * i : 8 * i + 8].astype(BF16)

    pl.semaphore_wait(barrier, NZ + NQ - 1)

    def remote(src, dst, ss, rs, device):
        copy = pltpu.make_async_remote_copy(src, dst, ss, rs, device_id=device, device_id_type=MESH)
        copy.start()
        return copy

    hop1 = []
    for d in range(1, NZ):
        zd = lax.rem(z + d, NZ)
        device = (z_peer(d), t)
        hop1.append(remote(meta_ref.at[zd], recvm.at[d], sms.at[d], smr.at[d], device))
        hop1.append(remote(send1.at[zd], recv1.at[d], s1s.at[d], s1r.at[d], device))
    weights = [
        remote(gate_ref.at[0, theirs], wg.at[:, lanes], w_ss.at[0], w_rs.at[0], partner),
        remote(up_ref.at[0, theirs], wu.at[:, lanes], w_ss.at[1], w_rs.at[1], partner),
        remote(down_ref.at[0, :, theirs], wd.at[lanes], w_ss.at[2], w_rs.at[2], partner),
    ]
    recv1[0] = send1[z]
    recvm[0] = meta_ref[z]

    col = iota((2 * NZ * NQ, 128), 0)
    chan = iota((2 * NZ * NQ, 128), 1)
    want = lax.rem(col, 2) * NQ + col // (2 * NZ)
    expand = jnp.where(chan == want, 1.0, 0.0).astype(BF16)
    expand_w = jnp.where(chan == want + 2 * NQ, 1.0, 0.0).astype(BF16)
    same_t = lax.rem(iota((2 * NZ * NQ, 64), 0) // 2, NZ) == iota((2 * NZ * NQ, 64), 1) // 8
    same = lax.rem(iota((64, 2 * NZ * NQ), 1) // 2, NZ) == iota((64, 2 * NZ * NQ), 0) // 8

    for copy in hop1:
        copy.wait_recv()
    meta = recvm[...].reshape(64, 128)
    meta_hi = meta.astype(BF16)
    choose = jnp.where(same_t, nt_dot(expand, meta_hi), 0.0).astype(BF16)
    arrived = recv1[...].astype(F32).reshape(64, half).astype(BF16)
    picked = jnp.dot(choose, arrived, preferred_element_type=F32).astype(BF16)
    send2[...] = picked.reshape(NQ, 2 * NZ, half)

    hop2 = []
    for i, (a, b) in enumerate(plane, 1):
        q = q_of(a, b)
        hop2.append(remote(send2.at[q], recv2.at[i], s2s.at[i], s2r.at[i], (z * NQ + q, t)))
    recv2[0] = send2[me_q]

    meta_lo = (meta - meta_hi.astype(F32)).astype(BF16)
    weigh_hi = jnp.where(same, nt_dot(meta_hi, expand_w), 0.0).astype(BF16)
    weigh_lo = jnp.where(same, nt_dot(meta_lo, expand_w), 0.0).astype(BF16)

    for copy in local:
        copy.wait()
    for copy in weights:
        copy.wait_recv()
    for copy in hop2:
        copy.wait_recv()

    flat = recv2[...].reshape(2 * NZ * NQ, half)
    gate_part = jnp.dot(flat, wg[...], preferred_element_type=F32)
    part[0] = gate_part.astype(BF16)
    gate_copy = remote(part.at[0], partr.at[0], ps.at[0], pr.at[0], partner)
    up_part = jnp.dot(flat, wu[...], preferred_element_type=F32)
    part[1] = up_part.astype(BF16)
    up_copy = remote(part.at[1], partr.at[1], ps.at[1], pr.at[1], partner)
    gate_copy.wait_recv()
    gate_sum = gate_part + partr[0].astype(F32)
    gated = gate_sum / (1.0 + jnp.exp(-gate_sum))
    up_copy.wait_recv()
    hidden = (gated * (up_part + partr[1].astype(F32))).astype(BF16)
    result = jnp.dot(hidden, wd[...], preferred_element_type=F32).astype(BF16)
    res[...] = result.reshape(NQ, 2 * NZ, half)

    hop3 = []
    for i, (a, b) in enumerate(plane, 1):
        q = q_of(-a, -b)
        hop3.append(remote(res.at[i], ret.at[me_q], s3s.at[i], s3r.at[i], (z * NQ + q, t)))
    ret[me_q] = res[0]
    for copy in hop3:
        copy.wait_recv()
    results = ret[...].reshape(2 * NZ * NQ, half)
    summed = jnp.dot(weigh_hi, results, preferred_element_type=F32)
    summed += jnp.dot(weigh_lo, results, preferred_element_type=F32)
    for i in range(NZ):
        comb[i] = summed[8 * i : 8 * i + 8].astype(BF16)

    hop4 = []
    for d in range(1, NZ):
        hop4.append(remote(comb.at[d], back.at[z], s4s.at[d], s4r.at[d], (z_peer(-d), t)))
    back[z] = comb[0]
    for copy in hop4:
        copy.wait_recv()
    sums = back[...].astype(F32).reshape(64, half).astype(BF16)
    moe_out = jnp.dot(p1t_ref[...], sums, preferred_element_type=F32)
    out_ref[...] = (own_ref[...].astype(F32) + moe_out).astype(BF16)

    for copy in hop1 + weights + hop2 + [gate_copy, up_copy] + hop3 + hop4:
        copy.wait_send()


def exchange(p1, p1t, meta, source, own_half, gate, up, down):
    rows, half = source.shape
    fh = gate.shape[2]
    slots = 2 * NZ * NQ
    vmem = pl.BlockSpec(memory_space=pltpu.VMEM)
    hbm = pl.BlockSpec(memory_space=pl.ANY)
    dma = pltpu.SemaphoreType.DMA
    return pl.pallas_call(
        exchange_kernel,
        out_shape=jax.ShapeDtypeStruct((rows, half), BF16),
        in_specs=[vmem] * 5 + [hbm] * 3,
        out_specs=vmem,
        scratch_shapes=[
            pltpu.VMEM((half, 2 * fh), BF16),
            pltpu.VMEM((half, 2 * fh), BF16),
            pltpu.VMEM((2 * fh, half), BF16),
            pltpu.VMEM((NZ, 8, half), BF16),
            pltpu.VMEM((NZ, 8, half), BF16),
            pltpu.VMEM((NZ, 8, 128), F32),
            pltpu.VMEM((NQ, 2 * NZ, half), BF16),
            pltpu.VMEM((NQ, 2 * NZ, half), BF16),
            pltpu.VMEM((2, slots, 2 * fh), BF16),
            pltpu.VMEM((2, slots, 2 * fh), BF16),
            pltpu.VMEM((NQ, 2 * NZ, half), BF16),
            pltpu.VMEM((NQ, 2 * NZ, half), BF16),
            pltpu.VMEM((NZ, 8, half), BF16),
            pltpu.VMEM((NZ, 8, half), BF16),
            dma((3,)), dma((3,)), dma((3,)),
            dma((NZ,)), dma((NZ,)), dma((NZ,)), dma((NZ,)),
            dma((NQ,)), dma((NQ,)),
            dma((2,)), dma((2,)),
            dma((NQ,)), dma((NQ,)),
            dma((NZ,)), dma((NZ,)),
        ],
        compiler_params=pltpu.CompilerParams(
            collective_id=0, has_side_effects=True, vmem_limit_bytes=32 * 1024 * 1024
        ),
    )(p1, p1t, meta, source, own_half, gate, up, down)


def total_of_pieces(value, axis):
    tiles = lax.all_gather(value, axis)
    return tiles.sum(axis=0)


def shards(
    tokens_in, state_in, norm_mix, w_recept, w_key, w_value, decay_down, decay_up, decay_base,
    iclr_down, iclr_up, iclr_base, key_scale, key_mix, w_out, norm_moe, router_group,
    router_expert, routes, expert_gate, expert_up, expert_down,
):
    f32 = jnp.float32
    bf16 = jnp.bfloat16
    seq_count = tokens_in.shape[0]
    width_model = tokens_in.shape[1]
    heads_here = state_in.shape[1]
    head_size = state_in.shape[-1]
    half_width = width_model // lax.axis_size("tp")

    def split_heads(values):
        return values.astype(f32).reshape(values.shape[0], heads_here, head_size)

    normed = rms_scale(tokens_in, norm_mix)
    recept = jnp.dot(normed, w_recept, preferred_element_type=f32).astype(bf16)
    key_rows = jnp.dot(normed, w_key, preferred_element_type=f32).astype(bf16)
    value_rows = jnp.dot(normed, w_value, preferred_element_type=f32).astype(bf16)
    decay_low = jnp.tanh(jnp.dot(normed, decay_down, preferred_element_type=f32)).astype(bf16)
    iclr_low = jnp.dot(normed, iclr_down, preferred_element_type=f32).astype(bf16)
    log_rate = (
        -jax.nn.softplus(-(decay_base + jnp.dot(decay_low, decay_up, preferred_element_type=f32)))
        - 0.5
    )
    decays = jnp.exp(-jnp.exp(log_rate))
    learn_rate = jax.nn.sigmoid(iclr_base + jnp.dot(iclr_low, iclr_up, preferred_element_type=f32))
    recept_heads = split_heads(recept)
    key_heads = split_heads(key_rows)
    value_heads = split_heads(value_rows)
    rate_heads = split_heads(learn_rate)
    decay_heads = split_heads(decays)
    scaled = key_heads * key_scale.astype(f32).reshape(heads_here, head_size)
    unit_key = scaled * lax.rsqrt(jnp.sum(scaled * scaled, axis=-1, keepdims=True) + 1e-06)
    key_mod = key_heads * (
        1.0 + (rate_heads - 1.0) * key_mix.astype(f32).reshape(heads_here, head_size)
    )
    removed = jnp.einsum("shvk,shk->shv", state_in, unit_key)
    state_out = (
        state_in * decay_heads[:, :, None, :]
        - removed[..., None] * (unit_key * rate_heads)[:, :, None, :]
        + value_heads[..., None] * key_mod[:, :, None, :]
    )
    mixed = (
        jnp.einsum("shvk,shk->shv", state_out, recept_heads)
        .reshape(seq_count, heads_here * head_size)
        .astype(bf16)
    )
    partial_value = jnp.dot(mixed, w_out, preferred_element_type=f32)
    mixer_out = total_of_pieces(partial_value, "tp").astype(bf16)
    x_mid = (tokens_in.astype(f32) + mixer_out.astype(f32)).astype(bf16)
    start = lax.axis_index("tp") * half_width
    own_half = lax.dynamic_slice_in_dim(x_mid, start, half_width, 1)
    moe_in = rms_scale(x_mid, norm_moe)
    n_groups = router_group.shape[1]
    experts_all = router_expert.shape[1]
    group_size = experts_all // n_groups
    group_id = routes[:, 0] // group_size
    group_logit = jnp.dot(moe_in, router_group, preferred_element_type=f32)
    group_hit = group_id[:, None] == jnp.arange(n_groups)[None, :]
    group_prob = jax.nn.sigmoid(jnp.sum(jnp.where(group_hit, group_logit, 0.0), axis=1))
    expert_logit = jnp.dot(moe_in, router_expert, preferred_element_type=f32)
    expert_hit = routes[:, :, None] == jnp.arange(experts_all)[None, None, :]
    scores = jax.nn.sigmoid(jnp.sum(jnp.where(expert_hit, expert_logit[:, None, :], 0.0), axis=2))
    route_weight = group_prob[:, None] * scores / jnp.sum(scores, axis=1, keepdims=True)

    order = jnp.arange(seq_count)
    named_before = jnp.sum(
        (routes[:, :, None, None] == routes[None, None, :, :]) & (order[:, None] > order)[:, None, :, None],
        axis=(2, 3),
    )
    rank = jnp.sum((group_id[:, None] == group_id[None, :]) & (order[:, None] > order[None, :]), axis=1)
    slot = group_id * 4 + rank
    p1t = slot[:, None] == jnp.arange(64)[None, :]
    channel = named_before * NQ + routes % NQ
    chans = jnp.arange(128)[None, None, :]
    tok_meta = jnp.sum(
        jnp.where(channel[:, :, None] == chans, 1.0, 0.0)
        + jnp.where(channel[:, :, None] + 2 * NQ == chans, route_weight[:, :, None], 0.0),
        axis=1,
    )
    p1 = p1t.T
    meta = jnp.dot(p1.astype(f32), tok_meta, precision=lax.Precision.HIGHEST).reshape(NZ, 8, 128)
    source = lax.dynamic_slice_in_dim(moe_in, start, half_width, 1)
    layer_out = exchange(
        p1.astype(bf16), p1t.astype(bf16), meta, source, own_half, expert_gate, expert_up, expert_down
    )
    return (layer_out, state_out)


def solution(mesh):
    in_specs = (
        P("ep", None),
        P("ep", "tp", None, None),
        P(),
        P(None, "tp"),
        P(None, "tp"),
        P(None, "tp"),
        P(),
        P(None, "tp"),
        P("tp"),
        P(),
        P(None, "tp"),
        P("tp"),
        P("tp"),
        P("tp"),
        P("tp", None),
        P(),
        P(),
        P(),
        P("ep", None),
        P("ep", None, "tp"),
        P("ep", None, "tp"),
        P("ep", "tp", None),
    )
    out_specs = (P("ep", "tp"), P("ep", "tp", None, None))
    return jax.shard_map(shards, mesh=mesh, in_specs=in_specs, out_specs=out_specs, check_vma=False)
```

time: 107 us -> 72 us (0.67)
  blocking collectives: 49.3 us -> 5 us
  Pallas kernels: 0 us -> 40.7 us
  waiting for transfers between devices: 18.5 us -> 0 us
  local copies, waits for them, and re-layouts: 9.4 us -> 2.78 us
  starting transfers between devices: 6.17 us -> 0 us
  other arithmetic: 7.83 us -> 9.3 us
  matrix products: 13.9 us -> 12.8 us
    all_to_all x3 -> x0, blocking collectives: 44.2 us -> none  [the longest x1 32.4 us: shards(): lax.all_to_all(outgoing, 'ep', split_axis=0, concat_axis=0, tiled=True)]
    pallas_call x0 -> x1, Pallas kernels: none -> 40.7 us  [exchange(): pl.pallas_call(exchange_kernel, out_shape=jax.ShapeDtypeStruct((rows, hal...]
    all_to_all x1 -> x0, waiting for transfers between devices: 18.5 us -> none  [shards(): lax.all_to_all(result, 'ep', split_axis=0, concat_axis=0, tiled=True)]
    all_to_all x1 -> x0, starting transfers between devices: 6.17 us -> none  [shards(): lax.all_to_all(result, 'ep', split_axis=0, concat_axis=0, tiled=True)]
    add x1, other arithmetic: 2.75 us -> 5.97 us  [shards(): state_in * decay_heads[:, :, None, :]]
    unnamed x28 -> x27, local copies, waits for them, and re-layouts: 3.1 us -> 0.71 us
    dot_general x1, matrix products: 1.17 us -> 3.48 us  [shards(): jnp.einsum('shvk,shk->shv', state_out, recept_heads)]
    dot_general x5 -> x1, matrix products: 1.87 us -> 0.2 us  [shards(): jnp.dot(p1.astype(f32), tok_meta, precision=lax.Precision.HIGHEST)]
  transfers between devices with their start and end apart: 1 -> 0, of which waited for: 1 -> 0; matrix products, arithmetic and copies ran while one was open for 1% -> 0% of each run, Pallas kernels for 0% -> 0%
where the time goes in v1:
time: 72 us; the launch traced here: 71.6 us
  Pallas kernels  40.7 us (57%)
  matrix products  12.8 us (18%)
  other arithmetic  9.3 us (13%)
  blocking collectives  5 us (7%)
  local copies, waits for them, and re-layouts  2.78 us (4%)
  between operations  1.01 us (1%)
    pallas_call x1, Pallas kernels, exchange(): pl.pallas_call(exchange_kernel, out_shape=jax.ShapeDtypeStruct((rows, hal...  40.7 us
    add x1, other arithmetic, shards(): state_in * decay_heads[:, :, None, :]  5.97 us
    all_gather x1, blocking collectives, total_of_pieces(): tiles = lax.all_gather(value, axis)  5 us
    dot_general x1, matrix products, shards(): jnp.einsum('shvk,shk->shv', state_out, recept_heads)  3.48 us
    dot_general x1, matrix products, shards(): removed = jnp.einsum('shvk,shk->shv', state_in, unit_key)  3.36 us
    dot_general x1, matrix products, shards(): key_rows = jnp.dot(normed, w_key, preferred_element_type=f32).astype(bf16)  1.63 us

profile of v1, /device:TPU:1, one launch (start us, length us, event | category | flops | bytes accessed | tf_op | source)
XLA Modules:
  0.0 71.6 jit_solution(10535800325327913452)
XLA Ops:
  0.7 0.8 %convert_element_type.72 = f32[2048]{0:T(1024)S(1)} convert(bf16[2048]{0:T(1024)(128)(2,1)} %param.24) | non-fusion elementwise | flops 2048 | bytes 12288 | tf_op jit(solution)/shard_map/convert_element_type | solution.py:18
  1.5 1.0 %fusion.12 = f32[32]{0:T(128)S(1)} fusion(bf16[32,2048]{1,0:T(8,128)(2,1)} %param.22), kind=kLoop, calls=%fused_computation.26 | loop fusion | flops 196576 | bytes 131200 | tf_op jit(solution)/shard_map/reduce_sum | solution.py:17
  2.6 1.6 %fusion.6 = f32[32,256]{1,0:T(8,128)S(1)} fusion(bf16[2048,256]{1,0:T(8,128)(2,1)} %param.26, bf16[32,2048]{1,0:T(8,128)(2,1)} %param.22, f32[2048]{0:T(1024)S(1)} %convert_element_type.72, f32[32]{0:T(128)S(1)} %add_rsqrt_fusion.2), kind=kOutput, calls=%fused_computation.12 | convolution fusion | flops 33832960 | bytes 1220736 | tf_op jit(solution)/shard_map/dot_general | solution.py:233
  4.3 0.7 %reshape.185 = f32[4,64]{1,0:T(4,128)S(1)} reshape(bf16[256]{0:T(256)(128)(2,1)} %param.34) | data formatting | bytes 1536 | tf_op jit(solution)/shard_map/mul | solution.py:248
  5.2 1.4 %fusion.3 = f32[32,256]{1,0:T(8,128)S(1)} fusion(bf16[64,256]{1,0:T(8,128)(2,1)} %param.32, bf16[2048,64]{0,1:T(8,128)(2,1)} %param.31, f32[256]{0:T(256)} %param.33, bf16[32,2048]{1,0:T(8,128)(2,1)} %param.22, f32[2048]{0:T(1024)S(1)} %convert_element_type.72, f32[32]{0:T(128)S(1)} %add_rsqrt_fusion.2), kind=kOutput, calls=%fused_computation.5 | convolution fusion | flops 9734144 | bytes 468096 | tf_op jit(solution)/shard_map/dot_general | solution.py:242
  6.7 0.7 %reshape.187 = f32[4,64]{1,0:T(4,128)S(1)} reshape(bf16[256]{0:T(256)(128)(2,1)} %param.35) | data formatting | bytes 1536 | tf_op jit(solution)/shard_map/mul | solution.py:251
  7.5 3.4 %fusion.42 = f32[32,4,1,64]{3,2,1,0:T(1,128)S(1)} fusion(f32[32,4,64,1]{2,3,1,0:T(1,128)S(1)} %bitcast.47, f32[32,4,64,64]{3,2,1,0:T(8,128)} %param.23), kind=kOutput, calls=%fused_computation.85 | convolution fusion | flops 1048576 | bytes 2162688 | tf_op jit(solution)/shard_map/shvk,shk->shv/dot_general | solution.py:253
  10.9 0.4 fusion.20
  11.5 0.3 fusion.5
  11.9 6.0 %multiply_add_fusion = f32[32,4,64,64]{3,2,1,0:T(8,128)} fusion(f32[32,4,64,64]{3,2,1,0:T(8,128)} %param.23, f32[32,4,64]{2,1,0:T(4,128)S(1)} %get-tuple-element.8, f32[32,4,64]{2,1,0:T(4,128)S(1)} %reshape.186, f32[32,4,64]{2,1,0:T(4,128)S(1)} %get-tuple-element.6, f32[32,4,64]{2,1,0:T(4,128)S(1)} %bitcast.45, f32[32,4,64]{2,1,0:T(4,128)S(1)} %mul.179), kind=kLoop, calls=%fused_computation | loop fusion | flops 2621440 | bytes 4358144 | tf_op jit(solution)/shard_map/add | solution.py:255
  17.9 0.3 convolution_convert_fusion
  18.4 3.5 %fusion.43 = f32[32,4,1,64]{3,2,1,0:T(1,128)S(1)} fusion(f32[32,4,64,64]{3,2,1,0:T(8,128)} %multiply_add_fusion, bf16[32,4,64,1]{2,3,1,0:T(2,128)(2,1)S(1)} %reshape.195), kind=kOutput, calls=%fused_computation.86 | convolution fusion | flops 1048576 | bytes 2146304 | tf_op jit(solution)/shard_map/shvk,shk->shv/dot_general | solution.py:260
  22.0 0.3 fusion.44
  22.3 5.0 %all-gather = f32[64,2048]{1,0:T(8,128)S(1)} all-gather(f32[32,2048]{1,0:T(8,128)S(1)} %fusion.44), channel_id=2, replica_groups=mesh['ep'=128,'tp'=2] {'tp'}, dimensions={0}, use_global_device_ids=true | all-gather | bytes 786432 | tf_op jit(solution)/shard_map/all_gather | solution.py:211
  27.3 0.2 fusion.9
  27.6 1.2 %fusion.45 = f32[32,128]{1,0:T(8,128)S(1)} fusion(bf16[32,2048]{1,0:T(8,128)(2,1)S(1)} %fusion.11, bf16[2048,128]{1,0:T(8,128)(2,1)} %param.39), kind=kOutput, calls=%fused_computation.88 | convolution fusion | flops 16777216 | bytes 671744 | tf_op jit(solution)/shard_map/dot_general | solution.py:277
  28.9 0.2 select_reduce_fusion
  29.1 0.2 fusion.8
  29.3 0.2 convert_reduce_fusion
  29.6 0.1 add_reduce_fusion
  29.8 0.2 convert_reduce_fusion.1
  30.0 0.2 fusion.22.meta_ref
  30.3 40.7 %shard_map.221 = bf16[32,1024]{1,0:T(8,128)(2,1)S(1)} custom-call(bf16[64,32]{1,0:T(8,128)(2,1)S(1)} %fusion.21.p1_ref, bf16[32,64]{1,0:T(8,128)(2,1)S(1)} %fusion.27.p1t_ref, f32[8,8,128]{2,1,0:T(8,128)S(1)} %fusion.22.meta_ref, bf16[32,1024]{1,0:T(8,128)(2,1)S(1)} %get-tuple-element.10.src_ref, bf16[32,1024]{1,0:T(8,128)(2,1)S(1)} %get-tuple-element.9.own_ref, ...), custom_call_target="tpu_custom_call" | custom-call | tf_op jit(solution)/shard_map/pallas_call | solution.py:177
  71.0 0.6 copy.34
  (53 shorter events, 1.3 us)
Async XLA Ops:
  0.6 21.4 %copy-start = (bf16[256,2048]{1,0:T(8,128)(2,1)S(1)}, bf16[256,2048]{1,0:T(8,128)(2,1)}, u32[]{:S(2)}) copy-start(bf16[256,2048]{1,0:T(8,128)(2,1)} %param.36) | copy-start | bytes 3145732
  0.6 10.2 %copy-start.4 = (bf16[32,2048]{1,0:T(8,128)(2,1)S(1)}, bf16[32,2048]{1,0:T(8,128)(2,1)}, u32[]{:S(2)}) copy-start(bf16[32,2048]{1,0:T(8,128)(2,1)} %param.22) | copy-start | bytes 393220
  0.7 10.2 %copy-start.10 = (bf16[2048,64]{0,1:T(8,128)(2,1)S(1)}, bf16[2048,64]{0,1:T(8,128)(2,1)}, u32[]{:S(2)}) copy-start(bf16[2048,64]{0,1:T(8,128)(2,1)} %param.28) | copy-start | bytes 786436
  0.7 10.2 %copy-start.11 = (bf16[64,256]{1,0:T(8,128)(2,1)S(1)}, bf16[64,256]{1,0:T(8,128)(2,1)}, u32[]{:S(2)}) copy-start(bf16[64,256]{1,0:T(8,128)(2,1)} %param.29) | copy-start | bytes 98308
  0.7 10.2 %copy-start.12 = (f32[256]{0:T(256)S(1)}, f32[256]{0:T(256)}, u32[]{:S(2)}) copy-start(f32[256]{0:T(256)} %param.30) | copy-start | bytes 3076
  0.7 10.8 %copy-start.5 = (bf16[2048,256]{1,0:T(8,128)(2,1)S(1)}, bf16[2048,256]{1,0:T(8,128)(2,1)}, u32[]{:S(2)}) copy-start(bf16[2048,256]{1,0:T(8,128)(2,1)} %param.27) | copy-start | bytes 3145732
  11.9 6.0 %copy-start.6 = (bf16[2048,256]{1,0:T(8,128)(2,1)S(1)}, bf16[2048,256]{1,0:T(8,128)(2,1)}, u32[]{:S(2)}) copy-start(bf16[2048,256]{1,0:T(8,128)(2,1)} %param.25) | copy-start | bytes 3145732
  17.9 9.6 %copy-start.9 = (bf16[2048]{0:T(1024)(128)(2,1)S(1)}, bf16[2048]{0:T(1024)(128)(2,1)}, u32[]{:S(2)}) copy-start(bf16[2048]{0:T(1024)(128)(2,1)} %param.37) | copy-start | bytes 12292
  18.3 10.6 %copy-start.8 = (s32[32,4]{0,1:T(4,128)S(1)}, s32[32,4]{0,1:T(4,128)}, u32[]{:S(2)}) copy-start(s32[32,4]{0,1:T(4,128)} %param.40) | copy-start | bytes 1540
  18.3 10.8 %copy-start.7 = (bf16[2048,16]{0,1:T(8,128)(2,1)S(1)}, bf16[2048,16]{0,1:T(8,128)(2,1)}, u32[]{:S(2)}) copy-start(bf16[2048,16]{0,1:T(8,128)(2,1)} %param.38) | copy-start | bytes 196612
  18.4 11.9 %copy-start.1 = (bf16[1,2048,128]{2,1,0:T(8,128)(2,1)S(1)}, bf16[1,2048,128]{2,1,0:T(8,128)(2,1)}, u32[]{:S(2)}) copy-start(bf16[1,2048,128]{2,1,0:T(8,128)(2,1)} %gate_ref.1) | copy-start | bytes 1572868
  18.4 11.9 %copy-start.2 = (bf16[1,2048,128]{2,1,0:T(8,128)(2,1)S(1)}, bf16[1,2048,128]{2,1,0:T(8,128)(2,1)}, u32[]{:S(2)}) copy-start(bf16[1,2048,128]{2,1,0:T(8,128)(2,1)} %up_ref.1) | copy-start | bytes 1572868
  18.4 11.9 %copy-start.3 = (bf16[1,128,2048]{2,1,0:T(8,128)(2,1)S(1)}, bf16[1,128,2048]{2,1,0:T(8,128)(2,1)}, u32[]{:S(2)}) copy-start(bf16[1,128,2048]{2,1,0:T(8,128)(2,1)} %down_ref.1) | copy-start | bytes 1572868

commit v2 on v1

v2 whole, which is shorter than its diff:
```python
import math

import jax
import jax.numpy as jnp
from jax import lax
from jax.experimental import pallas as pl
from jax.experimental.pallas import tpu as pltpu
from jax.sharding import PartitionSpec as P

MESH = pl.DeviceIdType.MESH
F32 = jnp.float32
BF16 = jnp.bfloat16
NZ, NY, NX = 8, 4, 4
NQ = NY * NX


def iota(shape, dim):
    return lax.broadcasted_iota(jnp.int32, shape, dim)


def one_hot(where):
    return jnp.where(where, 1.0, 0.0).astype(BF16)


def nt_dot(a, b):
    return lax.dot_general(a, b, (((1,), (1,)), ((), ())), preferred_element_type=F32)


def scale_rows(values32, gain):
    mean = jnp.mean(values32 * values32, axis=-1, keepdims=True)
    return (values32 * lax.rsqrt(mean + 1e-06) * gain).astype(BF16)


def sigmoid(u):
    return 1.0 / (1.0 + jnp.exp(-u))


def split_dot(a, b):
    hi = a.astype(BF16)
    lo = (a - hi.astype(F32)).astype(BF16)
    return jnp.dot(hi, b, preferred_element_type=F32) + jnp.dot(lo, b, preferred_element_type=F32)


def front_kernel(
    tok_ref, norm_ref, wr_ref, wk_ref, wv_ref, dd_ref, du_ref, db_ref, id_ref, iu_ref, ib_ref,
    ks_ref, km_ref, wo_ref, state_ref,
    partial_ref, state_out_ref,
    tok, norm, wr, wk, wv, dd, du, db, idn, iu, ib, ks, km, wo, sin, sout, lhs, decay, tall,
    isem, ssem, osem,
):
    seqs, heads, hs, _ = state_ref.shape
    width = heads * hs
    chunk = 8
    chunks = seqs // chunk
    loads = {}
    order = [
        ("tok", tok_ref, tok), ("norm", norm_ref, norm), ("wk", wk_ref, wk), ("dd", dd_ref, dd), ("id", id_ref, idn),
        ("wv", wv_ref, wv), ("wr", wr_ref, wr), ("du", du_ref, du), ("db", db_ref, db), ("iu", iu_ref, iu),
        ("ib", ib_ref, ib), ("ks", ks_ref, ks), ("km", km_ref, km),
    ]
    for i, (name, src, dst) in enumerate(order):
        loads[name] = pltpu.make_async_copy(src, dst, isem.at[i])
        loads[name].start()
    states = []
    for c in range(chunks):
        rows = pl.ds(c * chunk, chunk)
        states.append(pltpu.make_async_copy(state_ref.at[rows], sin.at[rows], ssem.at[c]))
        states[c].start()
    loads["wo"] = pltpu.make_async_copy(wo_ref, wo, isem.at[len(order)])
    loads["wo"].start()

    def got(*names):
        for name in names:
            loads[name].wait()

    got("tok", "norm")
    normed = scale_rows(tok[...].astype(F32), norm[...].astype(F32).reshape(1, -1))

    def project(weight):
        return jnp.dot(normed, weight[...], preferred_element_type=F32).astype(BF16)

    got("wk")
    key = project(wk).astype(F32)
    got("dd", "id")
    decay_low = jnp.tanh(nt_dot(normed, dd[...])).astype(BF16)
    iclr_low = nt_dot(normed, idn[...]).astype(BF16)
    got("wv", "wr")
    value = project(wv)
    recept = project(wr)
    got("du", "db", "iu", "ib", "ks", "km")
    rate_in = db[...].reshape(1, -1) + jnp.dot(decay_low, du[...], preferred_element_type=F32)
    decays = jnp.exp(-math.exp(-0.5) * sigmoid(rate_in))
    learn = sigmoid(ib[...].reshape(1, -1) + jnp.dot(iclr_low, iu[...], preferred_element_type=F32))
    scaled = key * ks[...].astype(F32).reshape(1, -1)
    head_ones = jnp.where(iota((width, width), 0) // hs == iota((width, width), 1) // hs, 1.0, 0.0).astype(BF16)
    unit_key = scaled * lax.rsqrt(split_dot(scaled * scaled, head_ones) + 1e-06)
    key_mod = key * (1.0 + (learn - 1.0) * km[...].astype(F32).reshape(1, -1))

    def by_head(values):
        return jnp.concatenate([values[:, h * hs : (h + 1) * hs] for h in range(heads)], axis=0)

    pairs = heads * seqs
    decay[...] = by_head(decays)
    keys_u = by_head(unit_key).astype(BF16)
    right = jnp.concatenate([by_head(-unit_key * learn), by_head(key_mod)], axis=0).astype(BF16)
    reads = by_head(recept.astype(F32)).astype(BF16)
    pick = jnp.where(iota((seqs, pairs), 0) == lax.rem(iota((seqs, pairs), 1), seqs), 1.0, 0.0).astype(BF16)
    spread = lax.dot_general(value, pick, (((0,), (0,)), ((), ())), preferred_element_type=F32)

    lane = iota((hs, pairs), 1)
    tall[...] = jnp.zeros_like(tall)
    for c in range(chunks):
        states[c].wait()
        for s in range(c * chunk, (c + 1) * chunk):
            found = nt_dot(sin[s].reshape(width, hs).astype(BF16), keys_u)
            for h in range(heads):
                own = lane == h * seqs + s
                rows = slice(h * hs, (h + 1) * hs)
                lhs[s - c * chunk, rows, :pairs] = jnp.where(own, found[rows], 0.0).astype(BF16)
                lhs[s - c * chunk, rows, pairs:] = jnp.where(own, spread[rows], 0.0).astype(BF16)
        for s in range(c * chunk, (c + 1) * chunk):
            update = jnp.dot(lhs[s - c * chunk], right, preferred_element_type=F32)
            for h in range(heads):
                row = h * seqs + s
                sout[s, h] = sin[s, h] * decay[row : row + 1, :] + update[h * hs : (h + 1) * hs]
        rows = pl.ds(c * chunk, chunk)
        pltpu.make_async_copy(sout.at[rows], state_out_ref.at[rows], osem.at[c]).start()
        for s in range(c * chunk, (c + 1) * chunk):
            seen = nt_dot(sout[s].reshape(width, hs).astype(BF16), reads)
            for h in range(heads):
                rows = slice(h * hs, (h + 1) * hs)
                tall[rows] = jnp.where(lane == h * seqs + s, seen[rows], tall[rows])
    mixed = nt_dot(pick, tall[...].astype(BF16)).astype(BF16)
    got("wo")
    partial_ref[...] = jnp.dot(mixed, wo[...], preferred_element_type=F32)
    for c in range(chunks):
        rows = pl.ds(c * chunk, chunk)
        pltpu.make_async_copy(sout.at[rows], state_out_ref.at[rows], osem.at[c]).wait()


def front(tok, norm, wr, wk, wv, dd, du, db, idn, iu, ib, ks, km, wo, state):
    seqs, heads, hs, _ = state.shape
    width, pairs = heads * hs, heads * seqs
    hbm = pl.BlockSpec(memory_space=pltpu.HBM)
    args = (tok, norm, wr, wk, wv, dd, du, db, idn, iu, ib, ks, km, wo)
    return pl.pallas_call(
        front_kernel,
        out_shape=(
            jax.ShapeDtypeStruct(tok.shape, F32),
            jax.ShapeDtypeStruct(state.shape, F32),
        ),
        in_specs=[hbm] * 15,
        out_specs=(pl.BlockSpec(memory_space=pltpu.VMEM), hbm),
        scratch_shapes=[pltpu.VMEM(a.shape, a.dtype) for a in args]
        + [
            pltpu.VMEM(state.shape, F32),
            pltpu.VMEM(state.shape, F32),
            pltpu.VMEM((8, width, 2 * pairs), BF16),
            pltpu.VMEM((pairs, hs), F32),
            pltpu.VMEM((width, pairs), F32),
            pltpu.SemaphoreType.DMA((len(args),)),
            pltpu.SemaphoreType.DMA((seqs // 8,)),
            pltpu.SemaphoreType.DMA((seqs // 8,)),
        ],
        compiler_params=pltpu.CompilerParams(vmem_limit_bytes=67043328),
    )(*args, state)


def exchange_kernel(
    pieces_ref, tok_ref, norm_ref, rg_ref, re_ref, routes_ref, gate_ref, up_ref, down_ref,
    out_ref,
    pieces, tok, norm, rg, rex, routes, xm, moe,
    wg, wu, wd, sendc, recvc, send1, recv1, sendm, recvm, send2, recv2, part, partr, res, ret, comb, back,
    isem, wsem, w_ss, w_rs, scs, scr, s1s, s1r, sms, smr, s2s, s2r, ps, pr, s3s, s3r, s4s, s4r,
):
    seqs, half = out_ref.shape
    fh = gate_ref.shape[2]
    experts = re_ref.shape[1]
    groups = rg_ref.shape[0]
    e = lax.axis_index("ep")
    t = lax.axis_index("tp")
    z, y, x = e // NQ, lax.rem(e // NX, NY), lax.rem(e, NX)
    me_q = lax.rem(e, NQ)
    partner = (e, 1 - t)

    def z_peer(d):
        return lax.rem(z + d + NZ, NZ) * NQ + me_q

    def q_of(a, b):
        return lax.rem(y + a + NY, NY) * NX + lax.rem(x + b + NX, NX)

    plane = [(a, b) for a in range(NY) for b in range(NX) if a or b]

    barrier = pltpu.get_barrier_semaphore()
    pl.semaphore_signal(barrier, inc=1, device_id=partner, device_id_type=MESH)
    for d in range(1, NZ):
        pl.semaphore_signal(barrier, inc=1, device_id=(z_peer(d), t), device_id_type=MESH)
    for a, b in plane:
        pl.semaphore_signal(barrier, inc=1, device_id=(z * NQ + q_of(a, b), t), device_id_type=MESH)

    mine = pl.ds(pl.multiple_of(t * half, half), half)
    theirs = pl.ds(pl.multiple_of((1 - t) * half, half), half)
    lanes = pl.ds(pl.multiple_of(t * fh, fh), fh)
    local = [
        pltpu.make_async_copy(gate_ref.at[0, mine], wg.at[:, lanes], wsem.at[0]),
        pltpu.make_async_copy(up_ref.at[0, mine], wu.at[:, lanes], wsem.at[1]),
        pltpu.make_async_copy(down_ref.at[0, :, mine], wd.at[lanes], wsem.at[2]),
    ]
    loads = {}
    for i, (name, src, dst) in enumerate([
        ("routes", routes_ref, routes), ("pieces", pieces_ref, pieces), ("tok", tok_ref, tok), ("norm", norm_ref, norm),
        ("rex", re_ref, rex), ("rg", rg_ref, rg),
    ]):
        loads[name] = pltpu.make_async_copy(src, dst, isem.at[i])
        loads[name].start()
    for copy in local:
        copy.start()

    loads["routes"].wait()
    table = jnp.concatenate([routes[...].astype(F32), jnp.zeros_like(routes, F32)], axis=0).astype(BF16)
    named = nt_dot(one_hot(iota((seqs, seqs), 0) == iota((seqs, seqs), 1)), table)
    expert_lane = iota((seqs, experts), 1).astype(F32)
    hit = jnp.zeros((seqs, experts), F32)
    for k in range(routes.shape[0]):
        hit += jnp.where(named[:, k : k + 1] == expert_lane, 1.0, 0.0)
    earlier = one_hot(iota((seqs, seqs), 1) < iota((seqs, seqs), 0))
    first = jnp.where(jnp.dot(earlier, hit.astype(BF16), preferred_element_type=F32) < 0.5, hit, 0.0)
    fold_row = iota((2 * experts, 128), 0)
    fold = one_hot(iota((2 * experts, 128), 1) == (fold_row // experts) * NQ + lax.rem(fold_row, NQ))
    group_of = one_hot(iota((experts, groups), 0) // (experts // groups) == iota((experts, groups), 1))
    in_group = jnp.where(jnp.dot(hit.astype(BF16), group_of, preferred_element_type=F32) > 0.5, 1.0, 0.0)
    before = jnp.dot(earlier, in_group.astype(BF16), preferred_element_type=F32)
    slot = jnp.sum(in_group * (4.0 * iota((seqs, groups), 1).astype(F32) + before), axis=1, keepdims=True)
    p1t = one_hot(slot == iota((seqs, 64), 1).astype(F32))
    p1 = nt_dot(one_hot(iota((64, 64), 0) == iota((64, 64), 1)), p1t).astype(BF16)
    ranked = jnp.concatenate([first, hit - first], axis=1)
    choice = jnp.dot(ranked.astype(BF16), fold, preferred_element_type=F32).astype(BF16)
    choice = jnp.dot(p1, choice, preferred_element_type=F32)
    for i in range(NZ):
        sendc[i] = choice[8 * i : 8 * i + 8].astype(BF16)

    for name in ("pieces", "tok", "norm"):
        loads[name].wait()
    mixer_out = (pieces[0] + pieces[1]).astype(BF16)
    x_mid = (tok[...].astype(F32) + mixer_out.astype(F32)).astype(BF16)
    moe_in = scale_rows(x_mid.astype(F32), norm[...].astype(F32).reshape(1, -1))
    for i in range(2):
        xm[i] = x_mid[:, i * half : (i + 1) * half]
        moe[i] = moe_in[:, i * half : (i + 1) * half]
    rows = jnp.dot(p1, moe[t], preferred_element_type=F32)
    for i in range(NZ):
        send1[i] = rows[8 * i : 8 * i + 8].astype(BF16)

    pl.semaphore_wait(barrier, NZ + NQ - 1)

    def remote(src, dst, ss, rs, device):
        copy = pltpu.make_async_remote_copy(src, dst, ss, rs, device_id=device, device_id_type=MESH)
        copy.start()
        return copy

    hop1 = []
    for d in range(1, NZ):
        zd = lax.rem(z + d, NZ)
        hop1.append(remote(sendc.at[zd], recvc.at[d], scs.at[d], scr.at[d], (z_peer(d), t)))
        hop1.append(remote(send1.at[zd], recv1.at[d], s1s.at[d], s1r.at[d], (z_peer(d), t)))
    weights = [
        remote(gate_ref.at[0, theirs], wg.at[:, lanes], w_ss.at[0], w_rs.at[0], partner),
        remote(up_ref.at[0, theirs], wu.at[:, lanes], w_ss.at[1], w_rs.at[1], partner),
        remote(down_ref.at[0, :, theirs], wd.at[lanes], w_ss.at[2], w_rs.at[2], partner),
    ]
    recvc[0] = sendc[z]
    recv1[0] = send1[z]

    loads["rex"].wait()
    loads["rg"].wait()
    scores = hit * sigmoid(jnp.dot(moe_in, rex[...], preferred_element_type=F32))
    group_prob = sigmoid(jnp.sum(in_group * nt_dot(moe_in, rg[...]), axis=1, keepdims=True))
    route_weight = group_prob * scores / jnp.sum(scores, axis=1, keepdims=True)
    weighed = jnp.concatenate([route_weight * first, route_weight * (hit - first)], axis=1)
    weighed = split_dot(weighed, fold)
    high = weighed.astype(BF16)
    low = (weighed - high.astype(F32)).astype(BF16)
    sendm[...] = (
        jnp.dot(p1, high, preferred_element_type=F32) + jnp.dot(p1, low, preferred_element_type=F32)
    ).reshape(NZ, 8, 128)
    hopw = []
    for d in range(1, NZ):
        zd = lax.rem(z + d, NZ)
        hopw.append(remote(sendm.at[zd], recvm.at[d], sms.at[d], smr.at[d], (z_peer(d), t)))
    recvm[0] = sendm[z]

    col = iota((2 * NZ * NQ, 128), 0)
    chan = iota((2 * NZ * NQ, 128), 1)
    want = lax.rem(col, 2) * NQ + col // (2 * NZ)
    expand = one_hot(chan == want)
    same_t = lax.rem(iota((2 * NZ * NQ, 64), 0) // 2, NZ) == iota((2 * NZ * NQ, 64), 1) // 8
    same = lax.rem(iota((64, 2 * NZ * NQ), 1) // 2, NZ) == iota((64, 2 * NZ * NQ), 0) // 8

    for copy in hop1:
        copy.wait_recv()
    chosen = recvc[...].astype(F32).reshape(64, 128).astype(BF16)
    choose = jnp.where(same_t, nt_dot(expand, chosen), 0.0).astype(BF16)
    arrived = recv1[...].astype(F32).reshape(64, half).astype(BF16)
    picked = jnp.dot(choose, arrived, preferred_element_type=F32).astype(BF16)
    send2[...] = picked.reshape(NQ, 2 * NZ, half)

    hop2 = []
    for i, (a, b) in enumerate(plane, 1):
        q = q_of(a, b)
        hop2.append(remote(send2.at[q], recv2.at[i], s2s.at[i], s2r.at[i], (z * NQ + q, t)))
    recv2[0] = send2[me_q]

    for copy in hopw:
        copy.wait_recv()
    meta = recvm[...].reshape(64, 128)
    meta_hi = meta.astype(BF16)
    meta_lo = (meta - meta_hi.astype(F32)).astype(BF16)
    weigh_hi = jnp.where(same, nt_dot(meta_hi, expand), 0.0).astype(BF16)
    weigh_lo = jnp.where(same, nt_dot(meta_lo, expand), 0.0).astype(BF16)

    for copy in local:
        copy.wait()
    for copy in weights:
        copy.wait_recv()
    for copy in hop2:
        copy.wait_recv()

    flat = recv2[...].reshape(2 * NZ * NQ, half)
    gate_part = jnp.dot(flat, wg[...], preferred_element_type=F32)
    part[0] = gate_part.astype(BF16)
    gate_copy = remote(part.at[0], partr.at[0], ps.at[0], pr.at[0], partner)
    up_part = jnp.dot(flat, wu[...], preferred_element_type=F32)
    part[1] = up_part.astype(BF16)
    up_copy = remote(part.at[1], partr.at[1], ps.at[1], pr.at[1], partner)
    gate_copy.wait_recv()
    gate_sum = gate_part + partr[0].astype(F32)
    gated = gate_sum / (1.0 + jnp.exp(-gate_sum))
    up_copy.wait_recv()
    hidden = (gated * (up_part + partr[1].astype(F32))).astype(BF16)
    result = jnp.dot(hidden, wd[...], preferred_element_type=F32).astype(BF16)
    res[...] = result.reshape(NQ, 2 * NZ, half)

    hop3 = []
    for i, (a, b) in enumerate(plane, 1):
        q = q_of(-a, -b)
        hop3.append(remote(res.at[i], ret.at[me_q], s3s.at[i], s3r.at[i], (z * NQ + q, t)))
    ret[me_q] = res[0]
    for copy in hop3:
        copy.wait_recv()
    results = ret[...].reshape(2 * NZ * NQ, half)
    summed = jnp.dot(weigh_hi, results, preferred_element_type=F32)
    summed += jnp.dot(weigh_lo, results, preferred_element_type=F32)
    for i in range(NZ):
        comb[i] = summed[8 * i : 8 * i + 8].astype(BF16)

    hop4 = []
    for d in range(1, NZ):
        hop4.append(remote(comb.at[d], back.at[z], s4s.at[d], s4r.at[d], (z_peer(-d), t)))
    back[z] = comb[0]
    for copy in hop4:
        copy.wait_recv()
    sums = back[...].astype(F32).reshape(64, half).astype(BF16)
    moe_out = jnp.dot(p1t, sums, preferred_element_type=F32)
    out_ref[...] = (xm[t].astype(F32) + moe_out).astype(BF16)

    for copy in hop1 + hopw + weights + hop2 + [gate_copy, up_copy] + hop3 + hop4:
        copy.wait_send()


def exchange(pieces, tok, norm, rg, rex, routes, gate, up, down):
    seqs, half = tok.shape[0], tok.shape[1] // 2
    fh = gate.shape[2]
    slots = 2 * NZ * NQ
    vmem = pl.BlockSpec(memory_space=pltpu.VMEM)
    hbm = pl.BlockSpec(memory_space=pl.ANY)
    dma = pltpu.SemaphoreType.DMA
    small = (pieces, tok, norm, rg, rex, routes)
    by_z = pltpu.VMEM((NZ, 8, half), BF16)
    by_q = pltpu.VMEM((NQ, 2 * NZ, half), BF16)
    return pl.pallas_call(
        exchange_kernel,
        out_shape=jax.ShapeDtypeStruct((seqs, half), BF16),
        in_specs=[hbm] * 9,
        out_specs=vmem,
        scratch_shapes=[pltpu.VMEM(a.shape, a.dtype) for a in small]
        + [
            pltpu.VMEM((2, seqs, half), BF16),
            pltpu.VMEM((2, seqs, half), BF16),
            pltpu.VMEM((half, 2 * fh), BF16),
            pltpu.VMEM((half, 2 * fh), BF16),
            pltpu.VMEM((2 * fh, half), BF16),
            pltpu.VMEM((NZ, 8, 128), BF16),
            pltpu.VMEM((NZ, 8, 128), BF16),
            by_z,
            by_z,
            pltpu.VMEM((NZ, 8, 128), F32),
            pltpu.VMEM((NZ, 8, 128), F32),
            by_q,
            by_q,
            pltpu.VMEM((2, slots, 2 * fh), BF16),
            pltpu.VMEM((2, slots, 2 * fh), BF16),
            by_q,
            by_q,
            by_z,
            by_z,
            dma((len(small),)),
            dma((3,)), dma((3,)), dma((3,)),
            dma((NZ,)), dma((NZ,)), dma((NZ,)), dma((NZ,)), dma((NZ,)), dma((NZ,)),
            dma((NQ,)), dma((NQ,)),
            dma((2,)), dma((2,)),
            dma((NQ,)), dma((NQ,)),
            dma((NZ,)), dma((NZ,)),
        ],
        compiler_params=pltpu.CompilerParams(
            collective_id=0, has_side_effects=True, vmem_limit_bytes=67043328
        ),
    )(*small, gate, up, down)


def shards(
    tokens_in, state_in, norm_mix, w_recept, w_key, w_value, decay_down, decay_up, decay_base,
    iclr_down, iclr_up, iclr_base, key_scale, key_mix, w_out, norm_moe, router_group,
    router_expert, routes, expert_gate, expert_up, expert_down,
):
    partial_value, state_out = front(
        tokens_in, norm_mix, w_recept, w_key, w_value, decay_down.T, decay_up, decay_base,
        iclr_down.T, iclr_up, iclr_base, key_scale, key_mix, w_out, state_in,
    )
    layer_out = exchange(
        lax.all_gather(partial_value, "tp"), tokens_in, norm_moe, router_group.T, router_expert, routes.T,
        expert_gate, expert_up, expert_down,
    )
    return (layer_out, state_out)


def solution(mesh):
    in_specs = (
        P("ep", None),
        P("ep", "tp", None, None),
        P(),
        P(None, "tp"),
        P(None, "tp"),
        P(None, "tp"),
        P(),
        P(None, "tp"),
        P("tp"),
        P(),
        P(None, "tp"),
        P("tp"),
        P("tp"),
        P("tp"),
        P("tp", None),
        P(),
        P(),
        P(),
        P("ep", None),
        P("ep", None, "tp"),
        P("ep", None, "tp"),
        P("ep", "tp", None),
    )
    out_specs = (P("ep", "tp"), P("ep", "tp", None, None))
    return jax.shard_map(shards, mesh=mesh, in_specs=in_specs, out_specs=out_specs, check_vma=False)
```

time: 72 us -> 58.1 us (0.81)
  matrix products: 12.8 us -> 0 us
  other arithmetic: 9.3 us -> 0 us
  Pallas kernels: 40.7 us -> 48.9 us
  blocking collectives: 5 us -> 6.88 us
  local copies, waits for them, and re-layouts: 2.78 us -> 1.47 us
    dot_general x11 -> x0, matrix products: 12.8 us -> none  [the longest x1 3.48 us: shards(): jnp.einsum('shvk,shk->shv', state_out, recept_heads)]
    pallas_call x1 -> x2, Pallas kernels: 40.7 us -> 48.9 us  [the longest x1 41.3 us: exchange(): pl.pallas_call(exchange_kernel, out_shape=jax.ShapeDtypeStruct((seqs, hal...]
    add x2 -> x0, other arithmetic: 5.99 us -> none  [the longest x1 5.97 us: shards(): state_in * decay_heads[:, :, None, :]]
    reduce_sum x9 -> x0, other arithmetic: 2.06 us -> none  [the longest x2 1.19 us: rms_scale(): jnp.mean(values32 * values32, axis=-1, keepdims=True) + 1e-06]
    all_gather x1, blocking collectives: 5 us -> 6.88 us  [shards(): lax.all_gather(partial_value, 'tp')]
    mul x4 -> x0, local copies, waits for them, and re-layouts: 1.67 us -> none  [the longest x1 0.74 us: shards(): scaled = key_heads * key_scale.astype(f32).reshape(heads_here, head_size)]
    convert_element_type x6 -> x0, other arithmetic: 1.06 us -> none  [the longest x2 0.84 us: rms_scale(): weights.astype(jnp.float32)]
    unnamed x27 -> x1, local copies, waits for them, and re-layouts: 0.71 us -> 1.47 us
where the time goes in v2:
time: 58.1 us; the launch traced here: 57.9 us
  Pallas kernels  48.9 us (84%)
  blocking collectives  6.88 us (12%)
  local copies, waits for them, and re-layouts  1.47 us (3%)
  between operations  0.65 us (1%)
    pallas_call x1, Pallas kernels, exchange(): pl.pallas_call(exchange_kernel, out_shape=jax.ShapeDtypeStruct((seqs, hal...  41.3 us
    pallas_call x1, Pallas kernels, front(): pl.pallas_call(front_kernel, out_shape=(jax.ShapeDtypeStruct(tok.shape, F...  7.56 us
    all_gather x1, blocking collectives, shards(): lax.all_gather(partial_value, 'tp')  6.88 us
    unnamed x1, local copies, waits for them, and re-layouts  1.47 us

profile of v2, /device:TPU:1, one launch (start us, length us, event | category | flops | bytes accessed | tf_op | source)
XLA Modules:
  0.0 57.9 jit_solution(1882048716208974556)
XLA Ops:
  0.6 7.6 %shard_map.221 = (f32[32,2048]{1,0:T(8,128)}, f32[32,4,64,64]{3,2,1,0:T(8,128)}) custom-call(bf16[32,2048]{1,0:T(8,128)(2,1)} %tok_ref.3, bf16[2048]{0:T(1024)(128)(2,1)} %norm_ref.2, bf16[2048,256]{1,0:T(8,128)(2,1)} %wr_ref.1, bf16[2048,256]{1,0:T(8,128)(2,1)} %wk_ref.1, bf16[2048,256]{1,0:T(8,128)(2,1)} %wv_ref.1, bf16[64,2048]{1,0:T(8,128)(2,1)} %bitcast.6, ...), custom_call_target="tpu_custom_call" | custom-call | tf_op jit(solution)/shard_map/pallas_call | solution.py:146
  8.2 6.9 %all-gather = f32[64,2048]{1,0:T(8,128)} all-gather(f32[32,2048]{1,0:T(8,128)} %get-tuple-element.4), channel_id=2, replica_groups=mesh['ep'=128,'tp'=2] {'tp'}, dimensions={0}, use_global_device_ids=true | all-gather | bytes 786432 | tf_op jit(solution)/shard_map/all_gather | solution.py:430
  15.1 41.3 %shard_map.222 = bf16[32,1024]{1,0:T(8,128)(2,1)} custom-call(f32[2,32,2048]{2,1,0:T(8,128)} %bitcast.5, bf16[32,2048]{1,0:T(8,128)(2,1)} %tok_ref.3, bf16[2048]{0:T(1024)(128)(2,1)} %norm_ref.3, bf16[16,2048]{1,0:T(8,128)(2,1)} %bitcast.8, bf16[2048,128]{1,0:T(8,128)(2,1)} %re_ref.1, s32[4,32]{1,0:T(4,128)} %bitcast.9, bf16[1,2048,128]{2,1,0:T(8,128)(2,1)} %gate_ref.1, ...), custom_call_target="tpu_custom_call" | custom-call | tf_op jit(solution)/shard_map/pallas_call | solution.py:380
  56.4 1.5 %copy.25 = bf16[32,1024]{1,0:T(8,128)(2,1)} copy(bf16[32,1024]{1,0:T(8,128)(2,1)} %shard_map.222) | data formatting | bytes 131072

commit v3 on v2

--- a/solution.py
+++ b/solution.py
@@ -12,6 +12,8 @@
 BF16 = jnp.bfloat16
 NZ, NY, NX = 8, 4, 4
 NQ = NY * NX
+ORDER = (0, 1, 7, 2, 6, 3, 5, 4)
+BATCH = NZ // 2
 
 
 def iota(shape, dim):
@@ -167,11 +169,11 @@
 
 
 def exchange_kernel(
-    pieces_ref, tok_ref, norm_ref, rg_ref, re_ref, routes_ref, gate_ref, up_ref, down_ref,
+    partial_ref, tok_ref, norm_ref, rg_ref, re_ref, routes_ref, gate_ref, up_ref, down_ref,
     out_ref,
-    pieces, tok, norm, rg, rex, routes, xm, moe,
+    partial, tok, norm, rg, rex, routes, other, xm, moe,
     wg, wu, wd, sendc, recvc, send1, recv1, sendm, recvm, send2, recv2, part, partr, res, ret, comb, back,
-    isem, wsem, w_ss, w_rs, scs, scr, s1s, s1r, sms, smr, s2s, s2r, ps, pr, s3s, s3r, s4s, s4r,
+    isem, wsem, w_ss, w_rs, xs, xr, scs, scr, s1s, s1r, sms, smr, s2s, s2r, ps, pr, s3s, s3r, s4s, s4r,
 ):
     seqs, half = out_ref.shape
     fh = gate_ref.shape[2]
@@ -208,7 +210,7 @@
     ]
     loads = {}
     for i, (name, src, dst) in enumerate([
-        ("routes", routes_ref, routes), ("pieces", pieces_ref, pieces), ("tok", tok_ref, tok), ("norm", norm_ref, norm),
+        ("routes", routes_ref, routes), ("partial", partial_ref, partial), ("tok", tok_ref, tok), ("norm", norm_ref, norm),
         ("rex", re_ref, rex), ("rg", rg_ref, rg),
     ]):
         loads[name] = pltpu.make_async_copy(src, dst, isem.at[i])
@@ -239,11 +241,31 @@
     for i in range(NZ):
         sendc[i] = choice[8 * i : 8 * i + 8].astype(BF16)
 
-    for name in ("pieces", "tok", "norm"):
-        loads[name].wait()
-    mixer_out = (pieces[0] + pieces[1]).astype(BF16)
+    loads["partial"].wait()
+    pl.semaphore_wait(barrier, NZ + NQ - 1)
+
+    def remote(src, dst, ss, rs, device):
+        copy = pltpu.make_async_remote_copy(src, dst, ss, rs, device_id=device, device_id_type=MESH)
+        copy.start()
+        return copy
+
+    def along_z(src, dst, ss, rs, step):
+        return remote(src, dst, ss, rs, (z_peer(step), t))
+
+    sent = [remote(partial, other, xs.at[0], xr.at[0], partner)]
+    mixer_copy = sent[0]
+    choices = []
+    for p in range(1, NZ):
+        zd = lax.rem(z + ORDER[p], NZ)
+        choices.append(along_z(sendc.at[zd], recvc.at[p], scs.at[p], scr.at[p], ORDER[p]))
+    recvc[0] = sendc[z]
+    loads["tok"].wait()
+    loads["norm"].wait()
+    gain = norm[...].astype(F32).reshape(1, -1)
+    mixer_copy.wait_recv()
+    mixer_out = (partial[...] + other[...]).astype(BF16)
     x_mid = (tok[...].astype(F32) + mixer_out.astype(F32)).astype(BF16)
-    moe_in = scale_rows(x_mid.astype(F32), norm[...].astype(F32).reshape(1, -1))
+    moe_in = scale_rows(x_mid.astype(F32), gain)
     for i in range(2):
         xm[i] = x_mid[:, i * half : (i + 1) * half]
         moe[i] = moe_in[:, i * half : (i + 1) * half]
@@ -251,111 +273,116 @@
     for i in range(NZ):
         send1[i] = rows[8 * i : 8 * i + 8].astype(BF16)
 
-    pl.semaphore_wait(barrier, NZ + NQ - 1)
-
-    def remote(src, dst, ss, rs, device):
-        copy = pltpu.make_async_remote_copy(src, dst, ss, rs, device_id=device, device_id_type=MESH)
-        copy.start()
-        return copy
-
-    hop1 = []
-    for d in range(1, NZ):
-        zd = lax.rem(z + d, NZ)
-        hop1.append(remote(sendc.at[zd], recvc.at[d], scs.at[d], scr.at[d], (z_peer(d), t)))
-        hop1.append(remote(send1.at[zd], recv1.at[d], s1s.at[d], s1r.at[d], (z_peer(d), t)))
+    hop1 = [None]
+    for p in range(1, NZ):
+        zd = lax.rem(z + ORDER[p], NZ)
+        hop1.append(along_z(send1.at[zd], recv1.at[p], s1s.at[p], s1r.at[p], ORDER[p]))
+    recv1[0] = send1[z]
     weights = [
         remote(gate_ref.at[0, theirs], wg.at[:, lanes], w_ss.at[0], w_rs.at[0], partner),
         remote(up_ref.at[0, theirs], wu.at[:, lanes], w_ss.at[1], w_rs.at[1], partner),
         remote(down_ref.at[0, :, theirs], wd.at[lanes], w_ss.at[2], w_rs.at[2], partner),
     ]
-    recvc[0] = sendc[z]
-    recv1[0] = send1[z]
-
-    loads["rex"].wait()
-    loads["rg"].wait()
-    scores = hit * sigmoid(jnp.dot(moe_in, rex[...], preferred_element_type=F32))
-    group_prob = sigmoid(jnp.sum(in_group * nt_dot(moe_in, rg[...]), axis=1, keepdims=True))
-    route_weight = group_prob * scores / jnp.sum(scores, axis=1, keepdims=True)
-    weighed = jnp.concatenate([route_weight * first, route_weight * (hit - first)], axis=1)
-    weighed = split_dot(weighed, fold)
-    high = weighed.astype(BF16)
-    low = (weighed - high.astype(F32)).astype(BF16)
-    sendm[...] = (
-        jnp.dot(p1, high, preferred_element_type=F32) + jnp.dot(p1, low, preferred_element_type=F32)
-    ).reshape(NZ, 8, 128)
-    hopw = []
-    for d in range(1, NZ):
-        zd = lax.rem(z + d, NZ)
-        hopw.append(remote(sendm.at[zd], recvm.at[d], sms.at[d], smr.at[d], (z_peer(d), t)))
-    recvm[0] = sendm[z]
-
-    col = iota((2 * NZ * NQ, 128), 0)
-    chan = iota((2 * NZ * NQ, 128), 1)
-    want = lax.rem(col, 2) * NQ + col // (2 * NZ)
-    expand = one_hot(chan == want)
-    same_t = lax.rem(iota((2 * NZ * NQ, 64), 0) // 2, NZ) == iota((2 * NZ * NQ, 64), 1) // 8
-    same = lax.rem(iota((64, 2 * NZ * NQ), 1) // 2, NZ) == iota((64, 2 * NZ * NQ), 0) // 8
-
-    for copy in hop1:
+
+    picks = 2 * BATCH * NQ
+    inputs = 8 * BATCH
+    col = iota((picks, 128), 0)
+    expand = one_hot(iota((picks, 128), 1) == lax.rem(col, 2) * NQ + col // (2 * BATCH))
+    same_t = lax.rem(iota((picks, inputs), 0) // 2, BATCH) == iota((picks, inputs), 1) // 8
+    same = lax.rem(iota((inputs, picks), 1) // 2, BATCH) == iota((inputs, picks), 0) // 8
+    for copy in choices:
         copy.wait_recv()
-    chosen = recvc[...].astype(F32).reshape(64, 128).astype(BF16)
-    choose = jnp.where(same_t, nt_dot(expand, chosen), 0.0).astype(BF16)
-    arrived = recv1[...].astype(F32).reshape(64, half).astype(BF16)
-    picked = jnp.dot(choose, arrived, preferred_element_type=F32).astype(BF16)
-    send2[...] = picked.reshape(NQ, 2 * NZ, half)
-
     hop2 = []
-    for i, (a, b) in enumerate(plane, 1):
-        q = q_of(a, b)
-        hop2.append(remote(send2.at[q], recv2.at[i], s2s.at[i], s2r.at[i], (z * NQ + q, t)))
-    recv2[0] = send2[me_q]
+    for b in range(2):
+        group = slice(b * BATCH, (b + 1) * BATCH)
+        chosen = recvc[group].astype(F32).reshape(inputs, 128).astype(BF16)
+        choose = jnp.where(same_t, nt_dot(expand, chosen), 0.0).astype(BF16)
+        for copy in hop1[group]:
+            if copy is not None:
+                copy.wait_recv()
+        arrived = recv1[group].astype(F32).reshape(inputs, half).astype(BF16)
+        picked = jnp.dot(choose, arrived, preferred_element_type=F32)
+        send2[b] = picked.reshape(NQ, 2 * BATCH, half).astype(BF16)
+        copies = []
+        for i, (a, c) in enumerate(plane, 1):
+            q = q_of(a, c)
+            copies.append(remote(send2.at[b, q], recv2.at[b, i], s2s.at[b, i], s2r.at[b, i], (z * NQ + q, t)))
+        recv2[b, 0] = send2[b, me_q]
+        hop2.append(copies)
+        if b == 0:
+            loads["rex"].wait()
+            loads["rg"].wait()
+            scores = hit * sigmoid(jnp.dot(moe_in, rex[...], preferred_element_type=F32))
+            group_prob = sigmoid(jnp.sum(in_group * nt_dot(moe_in, rg[...]), axis=1, keepdims=True))
+            route_weight = group_prob * scores / jnp.sum(scores, axis=1, keepdims=True)
+            weighed = jnp.concatenate([route_weight * first, route_weight * (hit - first)], axis=1)
+            weighed = split_dot(weighed, fold)
+            high = weighed.astype(BF16)
+            low = (weighed - high.astype(F32)).astype(BF16)
+            sendm[...] = (
+                jnp.dot(p1, high, preferred_element_type=F32) + jnp.dot(p1, low, preferred_element_type=F32)
+            ).reshape(NZ, 8, 128)
+            hopw = []
+            for p in range(1, NZ):
+                zd = lax.rem(z + ORDER[p], NZ)
+                hopw.append(along_z(sendm.at[zd], recvm.at[p], sms.at[p], smr.at[p], ORDER[p]))
+            recvm[0] = sendm[z]
 
     for copy in hopw:
         copy.wait_recv()
-    meta = recvm[...].reshape(64, 128)
-    meta_hi = meta.astype(BF16)
-    meta_lo = (meta - meta_hi.astype(F32)).astype(BF16)
-    weigh_hi = jnp.where(same, nt_dot(meta_hi, expand), 0.0).astype(BF16)
-    weigh_lo = jnp.where(same, nt_dot(meta_lo, expand), 0.0).astype(BF16)
+    weigh = []
+    for b in range(2):
+        meta = recvm[b * BATCH : (b + 1) * BATCH].reshape(inputs, 128)
+        meta_hi = meta.astype(BF16)
+        meta_lo = (meta - meta_hi.astype(F32)).astype(BF16)
+        for half_meta in (meta_hi, meta_lo):
+            weigh.append(jnp.where(same, nt_dot(half_meta, expand), 0.0).astype(BF16))
 
     for copy in local:
         copy.wait()
     for copy in weights:
         copy.wait_recv()
-    for copy in hop2:
-        copy.wait_recv()
-
-    flat = recv2[...].reshape(2 * NZ * NQ, half)
-    gate_part = jnp.dot(flat, wg[...], preferred_element_type=F32)
-    part[0] = gate_part.astype(BF16)
-    gate_copy = remote(part.at[0], partr.at[0], ps.at[0], pr.at[0], partner)
-    up_part = jnp.dot(flat, wu[...], preferred_element_type=F32)
-    part[1] = up_part.astype(BF16)
-    up_copy = remote(part.at[1], partr.at[1], ps.at[1], pr.at[1], partner)
-    gate_copy.wait_recv()
-    gate_sum = gate_part + partr[0].astype(F32)
-    gated = gate_sum / (1.0 + jnp.exp(-gate_sum))
-    up_copy.wait_recv()
-    hidden = (gated * (up_part + partr[1].astype(F32))).astype(BF16)
-    result = jnp.dot(hidden, wd[...], preferred_element_type=F32).astype(BF16)
-    res[...] = result.reshape(NQ, 2 * NZ, half)
 
     hop3 = []
-    for i, (a, b) in enumerate(plane, 1):
-        q = q_of(-a, -b)
-        hop3.append(remote(res.at[i], ret.at[me_q], s3s.at[i], s3r.at[i], (z * NQ + q, t)))
-    ret[me_q] = res[0]
-    for copy in hop3:
-        copy.wait_recv()
-    results = ret[...].reshape(2 * NZ * NQ, half)
-    summed = jnp.dot(weigh_hi, results, preferred_element_type=F32)
-    summed += jnp.dot(weigh_lo, results, preferred_element_type=F32)
-    for i in range(NZ):
-        comb[i] = summed[8 * i : 8 * i + 8].astype(BF16)
+    for b in range(2):
+        for copy in hop2[b]:
+            copy.wait_recv()
+        flat = recv2[b].astype(F32).reshape(picks, half).astype(BF16)
+        gate_part = jnp.dot(flat, wg[...], preferred_element_type=F32)
+        part[b, 0] = gate_part.astype(BF16)
+        gate_copy = remote(part.at[b, 0], partr.at[b, 0], ps.at[b, 0], pr.at[b, 0], partner)
+        up_part = jnp.dot(flat, wu[...], preferred_element_type=F32)
+        part[b, 1] = up_part.astype(BF16)
+        up_copy = remote(part.at[b, 1], partr.at[b, 1], ps.at[b, 1], pr.at[b, 1], partner)
+        sent += [gate_copy, up_copy]
+        gate_copy.wait_recv()
+        gate_sum = gate_part + partr[b, 0].astype(F32)
+        gated = gate_sum * sigmoid(gate_sum)
+        up_copy.wait_recv()
+        hidden = (gated * (up_part + partr[b, 1].astype(F32))).astype(BF16)
+        result = jnp.dot(hidden, wd[...], preferred_element_type=F32)
+        res[b] = result.reshape(NQ, 2 * BATCH, half).astype(BF16)
+        copies = []
+        for i, (a, c) in enumerate(plane, 1):
+            q = q_of(-a, -c)
+            copies.append(remote(res.at[b, i], ret.at[b, me_q], s3s.at[b, i], s3r.at[b, i], (z * NQ + q, t)))
+        ret[b, me_q] = res[b, 0]
+        hop3.append(copies)
 
     hop4 = []
-    for d in range(1, NZ):
-        hop4.append(remote(comb.at[d], back.at[z], s4s.at[d], s4r.at[d], (z_peer(-d), t)))
+    for b in range(2):
+        for copy in hop3[b]:
+            copy.wait_recv()
+        results = ret[b].astype(F32).reshape(picks, half).astype(BF16)
+        summed = jnp.dot(weigh[2 * b], results, preferred_element_type=F32)
+        summed += jnp.dot(weigh[2 * b + 1], results, preferred_element_type=F32)
+        for k in range(BATCH):
+            p = b * BATCH + k
+            comb[p] = summed[8 * k : 8 * k + 8].astype(BF16)
+        for k in range(BATCH):
+            p = b * BATCH + k
+            if p:
+                hop4.append(along_z(comb.at[p], back.at[z], s4s.at[p], s4r.at[p], -ORDER[p]))
     back[z] = comb[0]
     for copy in hop4:
         copy.wait_recv()
@@ -363,29 +390,30 @@
     moe_out = jnp.dot(p1t, sums, preferred_element_type=F32)
     out_ref[...] = (xm[t].astype(F32) + moe_out).astype(BF16)
 
-    for copy in hop1 + hopw + weights + hop2 + [gate_copy, up_copy] + hop3 + hop4:
+    for copy in sent + choices + hop1[1:] + hopw + weights + hop2[0] + hop2[1] + hop3[0] + hop3[1] + hop4:
         copy.wait_send()
 
 
-def exchange(pieces, tok, norm, rg, rex, routes, gate, up, down):
+def exchange(partial, tok, norm, rg, rex, routes, gate, up, down):
     seqs, half = tok.shape[0], tok.shape[1] // 2
     fh = gate.shape[2]
-    slots = 2 * NZ * NQ
-    vmem = pl.BlockSpec(memory_space=pltpu.VMEM)
     hbm = pl.BlockSpec(memory_space=pl.ANY)
     dma = pltpu.SemaphoreType.DMA
-    small = (pieces, tok, norm, rg, rex, routes)
+    small = (partial, tok, norm, rg, rex, routes)
+    by_half = pltpu.VMEM((2, seqs, half), BF16)
     by_z = pltpu.VMEM((NZ, 8, half), BF16)
-    by_q = pltpu.VMEM((NQ, 2 * NZ, half), BF16)
+    by_q = pltpu.VMEM((2, NQ, 2 * BATCH, half), BF16)
+    parts = pltpu.VMEM((2, 2, 2 * BATCH * NQ, 2 * fh), BF16)
     return pl.pallas_call(
         exchange_kernel,
         out_shape=jax.ShapeDtypeStruct((seqs, half), BF16),
         in_specs=[hbm] * 9,
-        out_specs=vmem,
+        out_specs=pl.BlockSpec(memory_space=pltpu.VMEM),
         scratch_shapes=[pltpu.VMEM(a.shape, a.dtype) for a in small]
         + [
-            pltpu.VMEM((2, seqs, half), BF16),
-            pltpu.VMEM((2, seqs, half), BF16),
+            pltpu.VMEM(partial.shape, F32),
+            by_half,
+            by_half,
             pltpu.VMEM((half, 2 * fh), BF16),
             pltpu.VMEM((half, 2 * fh), BF16),
             pltpu.VMEM((2 * fh, half), BF16),
@@ -397,18 +425,19 @@
             pltpu.VMEM((NZ, 8, 128), F32),
             by_q,
             by_q,
-            pltpu.VMEM((2, slots, 2 * fh), BF16),
-            pltpu.VMEM((2, slots, 2 * fh), BF16),
+            parts,
+            parts,
             by_q,
             by_q,
             by_z,
             by_z,
             dma((len(small),)),
             dma((3,)), dma((3,)), dma((3,)),
+            dma((1,)), dma((1,)),
             dma((NZ,)), dma((NZ,)), dma((NZ,)), dma((NZ,)), dma((NZ,)), dma((NZ,)),
-            dma((NQ,)), dma((NQ,)),
-            dma((2,)), dma((2,)),
-            dma((NQ,)), dma((NQ,)),
+            dma((2, NQ)), dma((2, NQ)),
+            dma((2, 2)), dma((2, 2)),
+            dma((2, NQ)), dma((2, NQ)),
             dma((NZ,)), dma((NZ,)),
         ],
         compiler_params=pltpu.CompilerParams(
@@ -427,7 +456,7 @@
         iclr_down.T, iclr_up, iclr_base, key_scale, key_mix, w_out, state_in,
     )
     layer_out = exchange(
-        lax.all_gather(partial_value, "tp"), tokens_in, norm_moe, router_group.T, router_expert, routes.T,
+        partial_value, tokens_in, norm_moe, router_group.T, router_expert, routes.T,
         expert_gate, expert_up, expert_down,
     )
     return (layer_out, state_out)

time: 58.1 us -> 51.2 us (0.88)
  blocking collectives: 6.88 us -> 0 us
    all_gather x1 -> x0, blocking collectives: 6.88 us -> none  [shards(): lax.all_gather(partial_value, 'tp')]
where the time goes in v3:
time: 51.2 us; the launch traced here: 50.6 us
  Pallas kernels  48.4 us (95%)
  local copies, waits for them, and re-layouts  1.47 us (3%)
  between operations  0.65 us (1%)
    pallas_call x1, Pallas kernels, exchange(): pl.pallas_call(exchange_kernel, out_shape=jax.ShapeDtypeStruct((seqs, hal...  40.9 us
    pallas_call x1, Pallas kernels, front(): pl.pallas_call(front_kernel, out_shape=(jax.ShapeDtypeStruct(tok.shape, F...  7.56 us
    unnamed x1, local copies, waits for them, and re-layouts  1.47 us

profile of v3, /device:TPU:1, one launch (start us, length us, event | category | flops | bytes accessed | tf_op | source)
XLA Modules:
  0.0 50.6 jit_solution(6729717890246493815)
XLA Ops:
  0.6 7.6 %shard_map.221 = (f32[32,2048]{1,0:T(8,128)}, f32[32,4,64,64]{3,2,1,0:T(8,128)}) custom-call(bf16[32,2048]{1,0:T(8,128)(2,1)} %tok_ref.3, bf16[2048]{0:T(1024)(128)(2,1)} %norm_ref.2, bf16[2048,256]{1,0:T(8,128)(2,1)} %wr_ref.1, bf16[2048,256]{1,0:T(8,128)(2,1)} %wk_ref.1, bf16[2048,256]{1,0:T(8,128)(2,1)} %wv_ref.1, bf16[64,2048]{1,0:T(8,128)(2,1)} %bitcast.4, ...), custom_call_target="tpu_custom_call" | custom-call | tf_op jit(solution)/shard_map/pallas_call | solution.py:148
  8.2 40.9 %shard_map.222 = bf16[32,1024]{1,0:T(8,128)(2,1)} custom-call(f32[32,2048]{1,0:T(8,128)} %get-tuple-element.4.partial_ref, bf16[32,2048]{1,0:T(8,128)(2,1)} %tok_ref.3, bf16[2048]{0:T(1024)(128)(2,1)} %norm_ref.3, bf16[16,2048]{1,0:T(8,128)(2,1)} %bitcast.6, bf16[2048,128]{1,0:T(8,128)(2,1)} %re_ref.1, s32[4,32]{1,0:T(4,128)} %bitcast.7, ...), custom_call_target="tpu_custom_call" | custom-call | tf_op jit(solution)/shard_map/pallas_call | solution.py:407
  49.1 1.5 %copy.25 = bf16[32,1024]{1,0:T(8,128)(2,1)} copy(bf16[32,1024]{1,0:T(8,128)(2,1)} %shard_map.222) | data formatting | bytes 131072

commit v4 on v3

--- a/solution.py
+++ b/solution.py
@@ -14,10 +14,23 @@
 NQ = NY * NX
 ORDER = (0, 1, 7, 2, 6, 3, 5, 4)
 BATCH = NZ // 2
+PIECE = 1
+PER = BATCH // PIECE
 
 
 def iota(shape, dim):
     return lax.broadcasted_iota(jnp.int32, shape, dim)
+
+
+def wait_for(name, region, sem):
+    with jax.named_scope(name):
+        pltpu.make_async_copy(region, region, sem).wait()
+
+
+def arrive(name, copies):
+    with jax.named_scope(name):
+        for copy in copies:
+            copy.wait_recv()
 
 
 def one_hot(where):
@@ -210,7 +223,7 @@
     ]
     loads = {}
     for i, (name, src, dst) in enumerate([
-        ("routes", routes_ref, routes), ("partial", partial_ref, partial), ("tok", tok_ref, tok), ("norm", norm_ref, norm),
+        ("partial", partial_ref, partial), ("routes", routes_ref, routes), ("tok", tok_ref, tok), ("norm", norm_ref, norm),
         ("rex", re_ref, rex), ("rg", rg_ref, rg),
     ]):
         loads[name] = pltpu.make_async_copy(src, dst, isem.at[i])
@@ -218,6 +231,20 @@
     for copy in local:
         copy.start()
 
+    with jax.named_scope("enter"):
+        loads["partial"].wait()
+        pl.semaphore_wait(barrier, NZ + NQ - 1)
+
+    def remote(src, dst, ss, rs, device):
+        copy = pltpu.make_async_remote_copy(src, dst, ss, rs, device_id=device, device_id_type=MESH)
+        copy.start()
+        return copy
+
+    def along_z(src, dst, ss, rs, step):
+        return remote(src, dst, ss, rs, (z_peer(step), t))
+
+    sent = [remote(partial, other, xs.at[0], xr.at[0], partner)]
+    mixer_copy = sent[0]
     loads["routes"].wait()
     table = jnp.concatenate([routes[...].astype(F32), jnp.zeros_like(routes, F32)], axis=0).astype(BF16)
     named = nt_dot(one_hot(iota((seqs, seqs), 0) == iota((seqs, seqs), 1)), table)
@@ -241,28 +268,14 @@
     for i in range(NZ):
         sendc[i] = choice[8 * i : 8 * i + 8].astype(BF16)
 
-    loads["partial"].wait()
-    pl.semaphore_wait(barrier, NZ + NQ - 1)
-
-    def remote(src, dst, ss, rs, device):
-        copy = pltpu.make_async_remote_copy(src, dst, ss, rs, device_id=device, device_id_type=MESH)
-        copy.start()
-        return copy
-
-    def along_z(src, dst, ss, rs, step):
-        return remote(src, dst, ss, rs, (z_peer(step), t))
-
-    sent = [remote(partial, other, xs.at[0], xr.at[0], partner)]
-    mixer_copy = sent[0]
-    choices = []
     for p in range(1, NZ):
         zd = lax.rem(z + ORDER[p], NZ)
-        choices.append(along_z(sendc.at[zd], recvc.at[p], scs.at[p], scr.at[p], ORDER[p]))
+        along_z(sendc.at[zd], recvc.at[p], scs, scr.at[p // PIECE], ORDER[p])
     recvc[0] = sendc[z]
     loads["tok"].wait()
     loads["norm"].wait()
     gain = norm[...].astype(F32).reshape(1, -1)
-    mixer_copy.wait_recv()
+    arrive("mixer", [mixer_copy])
     mixer_out = (partial[...] + other[...]).astype(BF16)
     x_mid = (tok[...].astype(F32) + mixer_out.astype(F32)).astype(BF16)
     moe_in = scale_rows(x_mid.astype(F32), gain)
@@ -273,10 +286,9 @@
     for i in range(NZ):
         send1[i] = rows[8 * i : 8 * i + 8].astype(BF16)
 
-    hop1 = [None]
     for p in range(1, NZ):
         zd = lax.rem(z + ORDER[p], NZ)
-        hop1.append(along_z(send1.at[zd], recv1.at[p], s1s.at[p], s1r.at[p], ORDER[p]))
+        along_z(send1.at[zd], recv1.at[p], s1s, s1r.at[p // PIECE], ORDER[p])
     recv1[0] = send1[z]
     weights = [
         remote(gate_ref.at[0, theirs], wg.at[:, lanes], w_ss.at[0], w_rs.at[0], partner),
@@ -284,96 +296,87 @@
         remote(down_ref.at[0, :, theirs], wd.at[lanes], w_ss.at[2], w_rs.at[2], partner),
     ]
 
-    picks = 2 * BATCH * NQ
-    inputs = 8 * BATCH
+    picks = 2 * PIECE * NQ
+    inputs = 8 * PIECE
     col = iota((picks, 128), 0)
-    expand = one_hot(iota((picks, 128), 1) == lax.rem(col, 2) * NQ + col // (2 * BATCH))
-    same_t = lax.rem(iota((picks, inputs), 0) // 2, BATCH) == iota((picks, inputs), 1) // 8
-    same = lax.rem(iota((inputs, picks), 1) // 2, BATCH) == iota((inputs, picks), 0) // 8
-    for copy in choices:
-        copy.wait_recv()
-    hop2 = []
-    for b in range(2):
-        group = slice(b * BATCH, (b + 1) * BATCH)
+    expand = one_hot(iota((picks, 128), 1) == lax.rem(col, 2) * NQ + col // (2 * PIECE))
+    same = lax.rem(iota((picks, inputs), 0) // 2, PIECE) == iota((picks, inputs), 1) // 8
+    for g in range(NZ // PIECE):
+        group = slice(g * PIECE, (g + 1) * PIECE)
+        came = pl.ds(max(1, g * PIECE), (g + 1) * PIECE - max(1, g * PIECE))
+        if came.size:
+            wait_for("choices", recvc.at[came], scr.at[g])
         chosen = recvc[group].astype(F32).reshape(inputs, 128).astype(BF16)
-        choose = jnp.where(same_t, nt_dot(expand, chosen), 0.0).astype(BF16)
-        for copy in hop1[group]:
-            if copy is not None:
-                copy.wait_recv()
+        choose = jnp.where(same, nt_dot(expand, chosen), 0.0).astype(BF16)
+        if came.size:
+            wait_for("hop1", recv1.at[came], s1r.at[g])
         arrived = recv1[group].astype(F32).reshape(inputs, half).astype(BF16)
         picked = jnp.dot(choose, arrived, preferred_element_type=F32)
-        send2[b] = picked.reshape(NQ, 2 * BATCH, half).astype(BF16)
-        copies = []
+        send2[g] = picked.reshape(NQ, 2 * PIECE, half).astype(BF16)
         for i, (a, c) in enumerate(plane, 1):
             q = q_of(a, c)
-            copies.append(remote(send2.at[b, q], recv2.at[b, i], s2s.at[b, i], s2r.at[b, i], (z * NQ + q, t)))
-        recv2[b, 0] = send2[b, me_q]
-        hop2.append(copies)
-        if b == 0:
-            loads["rex"].wait()
-            loads["rg"].wait()
-            scores = hit * sigmoid(jnp.dot(moe_in, rex[...], preferred_element_type=F32))
-            group_prob = sigmoid(jnp.sum(in_group * nt_dot(moe_in, rg[...]), axis=1, keepdims=True))
-            route_weight = group_prob * scores / jnp.sum(scores, axis=1, keepdims=True)
-            weighed = jnp.concatenate([route_weight * first, route_weight * (hit - first)], axis=1)
-            weighed = split_dot(weighed, fold)
-            high = weighed.astype(BF16)
-            low = (weighed - high.astype(F32)).astype(BF16)
-            sendm[...] = (
-                jnp.dot(p1, high, preferred_element_type=F32) + jnp.dot(p1, low, preferred_element_type=F32)
-            ).reshape(NZ, 8, 128)
-            hopw = []
-            for p in range(1, NZ):
-                zd = lax.rem(z + ORDER[p], NZ)
-                hopw.append(along_z(sendm.at[zd], recvm.at[p], sms.at[p], smr.at[p], ORDER[p]))
-            recvm[0] = sendm[z]
-
-    for copy in hopw:
-        copy.wait_recv()
+            remote(send2.at[g, q], recv2.at[g, i], s2s, s2r.at[g // PER], (z * NQ + q, t))
+        recv2[g, 0] = send2[g, me_q]
+
+    loads["rex"].wait()
+    loads["rg"].wait()
+    scores = hit * sigmoid(jnp.dot(moe_in, rex[...], preferred_element_type=F32))
+    group_prob = sigmoid(jnp.sum(in_group * nt_dot(moe_in, rg[...]), axis=1, keepdims=True))
+    route_weight = group_prob * scores / jnp.sum(scores, axis=1, keepdims=True)
+    weighed = jnp.concatenate([route_weight * first, route_weight * (hit - first)], axis=1)
+    weighed = split_dot(weighed, fold)
+    high = weighed.astype(BF16)
+    low = (weighed - high.astype(F32)).astype(BF16)
+    sendm[...] = (
+        jnp.dot(p1, high, preferred_element_type=F32) + jnp.dot(p1, low, preferred_element_type=F32)
+    ).reshape(NZ, 8, 128)
+    for p in range(1, NZ):
+        zd = lax.rem(z + ORDER[p], NZ)
+        along_z(sendm.at[zd], recvm.at[p], sms, smr, ORDER[p])
+    recvm[0] = sendm[z]
+
+    for copy in local:
+        copy.wait()
+    arrive("experts", weights)
+
+    for b in range(2):
+        wait_for("hop2", recv2.at[pl.ds(b * PER, PER), pl.ds(1, NQ - 1)], s2r.at[b])
+        flat = recv2[b * PER : (b + 1) * PER].astype(F32).reshape(PER * picks, half).astype(BF16)
+        gate_part = jnp.dot(flat, wg[...], preferred_element_type=F32)
+        part[b, 0] = gate_part.astype(BF16)
+        gate_copy = remote(part.at[b, 0], partr.at[b, 0], ps, pr.at[b, 0], partner)
+        up_part = jnp.dot(flat, wu[...], preferred_element_type=F32)
+        part[b, 1] = up_part.astype(BF16)
+        up_copy = remote(part.at[b, 1], partr.at[b, 1], ps, pr.at[b, 1], partner)
+        arrive("gate", [gate_copy])
+        gate_sum = gate_part + partr[b, 0].astype(F32)
+        gated = gate_sum * sigmoid(gate_sum)
+        arrive("up", [up_copy])
+        hidden = (gated * (up_part + partr[b, 1].astype(F32))).astype(BF16)
+        result = jnp.dot(hidden, wd[...], preferred_element_type=F32)
+        res[b] = result.reshape(PER, NQ, 2 * PIECE, half).astype(BF16)
+        for i, (a, c) in enumerate(plane, 1):
+            q = q_of(-a, -c)
+            remote(res.at[b, :, i], ret.at[b, :, me_q], s3s, s3r.at[b], (z * NQ + q, t))
+        for g in range(PER):
+            ret[b, g, me_q] = res[b, g, 0]
+
+    wait_for("weights", recvm.at[pl.ds(1, NZ - 1)], smr)
+    row = iota((8 * BATCH, PER * picks), 0) // 8
+    column = iota((8 * BATCH, PER * picks), 1)
+    own = row == column // picks * PIECE + lax.rem(column // 2, PIECE)
     weigh = []
     for b in range(2):
-        meta = recvm[b * BATCH : (b + 1) * BATCH].reshape(inputs, 128)
+        meta = recvm[b * BATCH : (b + 1) * BATCH].reshape(8 * BATCH, 128)
         meta_hi = meta.astype(BF16)
         meta_lo = (meta - meta_hi.astype(F32)).astype(BF16)
         for half_meta in (meta_hi, meta_lo):
-            weigh.append(jnp.where(same, nt_dot(half_meta, expand), 0.0).astype(BF16))
-
-    for copy in local:
-        copy.wait()
-    for copy in weights:
-        copy.wait_recv()
-
-    hop3 = []
+            spread = nt_dot(half_meta, expand)
+            weigh.append(jnp.where(own, jnp.concatenate([spread] * PER, axis=1), 0.0).astype(BF16))
+
     for b in range(2):
-        for copy in hop2[b]:
-            copy.wait_recv()
-        flat = recv2[b].astype(F32).reshape(picks, half).astype(BF16)
-        gate_part = jnp.dot(flat, wg[...], preferred_element_type=F32)
-        part[b, 0] = gate_part.astype(BF16)
-        gate_copy = remote(part.at[b, 0], partr.at[b, 0], ps.at[b, 0], pr.at[b, 0], partner)
-        up_part = jnp.dot(flat, wu[...], preferred_element_type=F32)
-        part[b, 1] = up_part.astype(BF16)
-        up_copy = remote(part.at[b, 1], partr.at[b, 1], ps.at[b, 1], pr.at[b, 1], partner)
-        sent += [gate_copy, up_copy]
-        gate_copy.wait_recv()
-        gate_sum = gate_part + partr[b, 0].astype(F32)
-        gated = gate_sum * sigmoid(gate_sum)
-        up_copy.wait_recv()
-        hidden = (gated * (up_part + partr[b, 1].astype(F32))).astype(BF16)
-        result = jnp.dot(hidden, wd[...], preferred_element_type=F32)
-        res[b] = result.reshape(NQ, 2 * BATCH, half).astype(BF16)
-        copies = []
-        for i, (a, c) in enumerate(plane, 1):
-            q = q_of(-a, -c)
-            copies.append(remote(res.at[b, i], ret.at[b, me_q], s3s.at[b, i], s3r.at[b, i], (z * NQ + q, t)))
-        ret[b, me_q] = res[b, 0]
-        hop3.append(copies)
-
-    hop4 = []
-    for b in range(2):
-        for copy in hop3[b]:
-            copy.wait_recv()
-        results = ret[b].astype(F32).reshape(picks, half).astype(BF16)
+        wait_for("hop3", ret.at[b, :, pl.ds(1, NQ - 1)], s3r.at[b])
+        results = ret[b].astype(F32).reshape(PER * picks, half).astype(BF16)
         summed = jnp.dot(weigh[2 * b], results, preferred_element_type=F32)
         summed += jnp.dot(weigh[2 * b + 1], results, preferred_element_type=F32)
         for k in range(BATCH):
@@ -382,16 +385,21 @@
         for k in range(BATCH):
             p = b * BATCH + k
             if p:
-                hop4.append(along_z(comb.at[p], back.at[z], s4s.at[p], s4r.at[p], -ORDER[p]))
+                along_z(comb.at[p], back.at[z], s4s, s4r, -ORDER[p])
     back[z] = comb[0]
-    for copy in hop4:
-        copy.wait_recv()
+    wait_for("hop4", back.at[pl.ds(1, NZ - 1)], s4r)
     sums = back[...].astype(F32).reshape(64, half).astype(BF16)
     moe_out = jnp.dot(p1t, sums, preferred_element_type=F32)
     out_ref[...] = (xm[t].astype(F32) + moe_out).astype(BF16)
 
-    for copy in sent + choices + hop1[1:] + hopw + weights + hop2[0] + hop2[1] + hop3[0] + hop3[1] + hop4:
+    for copy in sent + weights:
         copy.wait_send()
+    others = pl.ds(1, NZ - 1)
+    for region, sem in (
+        (sendc.at[others], scs), (send1.at[others], s1s), (sendm.at[others], sms), (comb.at[others], s4s),
+        (send2.at[:, pl.ds(1, NQ - 1)], s2s), (part, ps), (res.at[:, :, pl.ds(1, NQ - 1)], s3s),
+    ):
+        wait_for("sent", region, sem)
 
 
 def exchange(partial, tok, norm, rg, rex, routes, gate, up, down):
@@ -402,7 +410,9 @@
     small = (partial, tok, norm, rg, rex, routes)
     by_half = pltpu.VMEM((2, seqs, half), BF16)
     by_z = pltpu.VMEM((NZ, 8, half), BF16)
-    by_q = pltpu.VMEM((2, NQ, 2 * BATCH, half), BF16)
+    pieces = NZ // PIECE
+    in_q = pltpu.VMEM((pieces, NQ, 2 * PIECE, half), BF16)
+    out_q = pltpu.VMEM((2, PER, NQ, 2 * PIECE, half), BF16)
     parts = pltpu.VMEM((2, 2, 2 * BATCH * NQ, 2 * fh), BF16)
     return pl.pallas_call(
         exchange_kernel,
@@ -423,22 +433,22 @@
             by_z,
             pltpu.VMEM((NZ, 8, 128), F32),
             pltpu.VMEM((NZ, 8, 128), F32),
-            by_q,
-            by_q,
+            in_q,
+            in_q,
             parts,
             parts,
-            by_q,
-            by_q,
+            out_q,
+            out_q,
             by_z,
             by_z,
             dma((len(small),)),
             dma((3,)), dma((3,)), dma((3,)),
             dma((1,)), dma((1,)),
-            dma((NZ,)), dma((NZ,)), dma((NZ,)), dma((NZ,)), dma((NZ,)), dma((NZ,)),
-            dma((2, NQ)), dma((2, NQ)),
-            dma((2, 2)), dma((2, 2)),
-            dma((2, NQ)), dma((2, NQ)),
-            dma((NZ,)), dma((NZ,)),
+            dma, dma((pieces,)), dma, dma((pieces,)), dma, dma,
+            dma, dma((2,)),
+            dma, dma((2, 2)),
+            dma, dma((2,)),
+            dma, dma,
         ],
         compiler_params=pltpu.CompilerParams(
             collective_id=0, has_side_effects=True, vmem_limit_bytes=67043328

time: 51.2 us -> 48.5 us (0.947)
  Pallas kernels: 48.4 us -> 45.7 us
    pallas_call x1, Pallas kernels: 40.9 us -> 38.2 us  [exchange(): pl.pallas_call(exchange_kernel, out_shape=jax.ShapeDtypeStruct((seqs, hal...]
where the time goes in v4:
time: 48.5 us; the launch traced here: 47.9 us
  Pallas kernels  45.7 us (94%)
  local copies, waits for them, and re-layouts  1.47 us (3%)
  between operations  0.65 us (1%)
    pallas_call x1, Pallas kernels, exchange(): pl.pallas_call(exchange_kernel, out_shape=jax.ShapeDtypeStruct((seqs, hal...  38.2 us
    pallas_call x1, Pallas kernels, front(): pl.pallas_call(front_kernel, out_shape=(jax.ShapeDtypeStruct(tok.shape, F...  7.56 us
    unnamed x1, local copies, waits for them, and re-layouts  1.47 us

profile of v4, /device:TPU:1, one launch (start us, length us, event | category | flops | bytes accessed | tf_op | source)
XLA Modules:
  0.0 47.9 jit_solution(1579776507991945942)
XLA Ops:
  0.6 7.6 %shard_map.221 = (f32[32,2048]{1,0:T(8,128)}, f32[32,4,64,64]{3,2,1,0:T(8,128)}) custom-call(bf16[32,2048]{1,0:T(8,128)(2,1)} %tok_ref.3, bf16[2048]{0:T(1024)(128)(2,1)} %norm_ref.2, bf16[2048,256]{1,0:T(8,128)(2,1)} %wr_ref.1, bf16[2048,256]{1,0:T(8,128)(2,1)} %wk_ref.1, bf16[2048,256]{1,0:T(8,128)(2,1)} %wv_ref.1, bf16[64,2048]{1,0:T(8,128)(2,1)} %bitcast.4, ...), custom_call_target="tpu_custom_call" | custom-call | tf_op jit(solution)/shard_map/pallas_call | solution.py:161
  8.2 38.2 %shard_map.222 = bf16[32,1024]{1,0:T(8,128)(2,1)} custom-call(f32[32,2048]{1,0:T(8,128)} %get-tuple-element.4.partial_ref, bf16[32,2048]{1,0:T(8,128)(2,1)} %tok_ref.3, bf16[2048]{0:T(1024)(128)(2,1)} %norm_ref.3, bf16[16,2048]{1,0:T(8,128)(2,1)} %bitcast.6, bf16[2048,128]{1,0:T(8,128)(2,1)} %re_ref.1, s32[4,32]{1,0:T(4,128)} %bitcast.7, ...), custom_call_target="tpu_custom_call" | custom-call | tf_op jit(solution)/shard_map/pallas_call | solution.py:417
  46.4 1.5 %copy.25 = bf16[32,1024]{1,0:T(8,128)(2,1)} copy(bf16[32,1024]{1,0:T(8,128)(2,1)} %shard_map.222) | data formatting | bytes 131072

commit v5 on v4

--- a/solution.py
+++ b/solution.py
@@ -13,9 +13,9 @@
 NZ, NY, NX = 8, 4, 4
 NQ = NY * NX
 ORDER = (0, 1, 7, 2, 6, 3, 5, 4)
-BATCH = NZ // 2
-PIECE = 1
-PER = BATCH // PIECE
+PASSES = ((0, 2), (2, 4), (4, 6), (6, 8))
+FLIGHT = 1
+PASS_OF = tuple(k for k, (low, high) in enumerate(PASSES) for _ in range(low, high))
 
 
 def iota(shape, dim):
@@ -270,7 +270,7 @@
 
     for p in range(1, NZ):
         zd = lax.rem(z + ORDER[p], NZ)
-        along_z(sendc.at[zd], recvc.at[p], scs, scr.at[p // PIECE], ORDER[p])
+        along_z(sendc.at[zd], recvc.at[p], scs, scr.at[p], ORDER[p])
     recvc[0] = sendc[z]
     loads["tok"].wait()
     loads["norm"].wait()
@@ -288,7 +288,7 @@
 
     for p in range(1, NZ):
         zd = lax.rem(z + ORDER[p], NZ)
-        along_z(send1.at[zd], recv1.at[p], s1s, s1r.at[p // PIECE], ORDER[p])
+        along_z(send1.at[zd], recv1.at[p], s1s, s1r.at[p], ORDER[p])
     recv1[0] = send1[z]
     weights = [
         remote(gate_ref.at[0, theirs], wg.at[:, lanes], w_ss.at[0], w_rs.at[0], partner),
@@ -296,27 +296,21 @@
         remote(down_ref.at[0, :, theirs], wd.at[lanes], w_ss.at[2], w_rs.at[2], partner),
     ]
 
-    picks = 2 * PIECE * NQ
-    inputs = 8 * PIECE
-    col = iota((picks, 128), 0)
-    expand = one_hot(iota((picks, 128), 1) == lax.rem(col, 2) * NQ + col // (2 * PIECE))
-    same = lax.rem(iota((picks, inputs), 0) // 2, PIECE) == iota((picks, inputs), 1) // 8
-    for g in range(NZ // PIECE):
-        group = slice(g * PIECE, (g + 1) * PIECE)
-        came = pl.ds(max(1, g * PIECE), (g + 1) * PIECE - max(1, g * PIECE))
-        if came.size:
-            wait_for("choices", recvc.at[came], scr.at[g])
-        chosen = recvc[group].astype(F32).reshape(inputs, 128).astype(BF16)
-        choose = jnp.where(same, nt_dot(expand, chosen), 0.0).astype(BF16)
-        if came.size:
-            wait_for("hop1", recv1.at[came], s1r.at[g])
-        arrived = recv1[group].astype(F32).reshape(inputs, half).astype(BF16)
-        picked = jnp.dot(choose, arrived, preferred_element_type=F32)
-        send2[g] = picked.reshape(NQ, 2 * PIECE, half).astype(BF16)
+    picks = 2 * NQ
+    column = iota((picks, 128), 0)
+    expand = one_hot(iota((picks, 128), 1) == lax.rem(column, 2) * NQ + column // 2)
+    for p in range(NZ):
+        if p:
+            wait_for("choices", recvc.at[p], scr.at[p])
+        choose = nt_dot(expand, recvc[p]).astype(BF16)
+        if p:
+            wait_for("hop1", recv1.at[p], s1r.at[p])
+        picked = jnp.dot(choose, recv1[p], preferred_element_type=F32)
+        send2[p] = picked.reshape(NQ, 2, half).astype(BF16)
         for i, (a, c) in enumerate(plane, 1):
             q = q_of(a, c)
-            remote(send2.at[g, q], recv2.at[g, i], s2s, s2r.at[g // PER], (z * NQ + q, t))
-        recv2[g, 0] = send2[g, me_q]
+            remote(send2.at[p, q], recv2.at[p, i], s2s, s2r.at[PASS_OF[p]], (z * NQ + q, t))
+        recv2[p, 0] = send2[p, me_q]
 
     loads["rex"].wait()
     loads["rg"].wait()
@@ -339,51 +333,62 @@
         copy.wait()
     arrive("experts", weights)
 
-    for b in range(2):
-        wait_for("hop2", recv2.at[pl.ds(b * PER, PER), pl.ds(1, NQ - 1)], s2r.at[b])
-        flat = recv2[b * PER : (b + 1) * PER].astype(F32).reshape(PER * picks, half).astype(BF16)
-        gate_part = jnp.dot(flat, wg[...], preferred_element_type=F32)
-        part[b, 0] = gate_part.astype(BF16)
-        gate_copy = remote(part.at[b, 0], partr.at[b, 0], ps, pr.at[b, 0], partner)
-        up_part = jnp.dot(flat, wu[...], preferred_element_type=F32)
-        part[b, 1] = up_part.astype(BF16)
-        up_copy = remote(part.at[b, 1], partr.at[b, 1], ps, pr.at[b, 1], partner)
-        arrive("gate", [gate_copy])
-        gate_sum = gate_part + partr[b, 0].astype(F32)
+    others_q = pl.ds(1, NQ - 1)
+    def begin(b):
+        low, high = PASSES[b]
+        lines = pl.ds(low * picks, (high - low) * picks)
+        wait_for("hop2", recv2.at[pl.ds(low, high - low), others_q], s2r.at[b])
+        flat = recv2[low:high].astype(F32).reshape((high - low) * picks, half).astype(BF16)
+        copies, parts = [], []
+        for k, weight in enumerate((wg, wu)):
+            parts.append(jnp.dot(flat, weight[...], preferred_element_type=F32))
+            part[k, lines] = parts[k].astype(BF16)
+            copies.append(remote(part.at[k, lines], partr.at[k, lines], ps, pr.at[b, k], partner))
+        return copies, parts
+
+    def finish(b, copies, parts):
+        low, high = PASSES[b]
+        group = pl.ds(low, high - low)
+        lines = pl.ds(low * picks, (high - low) * picks)
+        arrive("gate", [copies[0]])
+        gate_sum = parts[0] + partr[0, lines].astype(F32)
         gated = gate_sum * sigmoid(gate_sum)
-        arrive("up", [up_copy])
-        hidden = (gated * (up_part + partr[b, 1].astype(F32))).astype(BF16)
+        arrive("up", [copies[1]])
+        hidden = (gated * (parts[1] + partr[1, lines].astype(F32))).astype(BF16)
         result = jnp.dot(hidden, wd[...], preferred_element_type=F32)
-        res[b] = result.reshape(PER, NQ, 2 * PIECE, half).astype(BF16)
+        res[low:high] = result.reshape(high - low, NQ, 2, half).astype(BF16)
         for i, (a, c) in enumerate(plane, 1):
             q = q_of(-a, -c)
-            remote(res.at[b, :, i], ret.at[b, :, me_q], s3s, s3r.at[b], (z * NQ + q, t))
-        for g in range(PER):
-            ret[b, g, me_q] = res[b, g, 0]
+            remote(res.at[group, i], ret.at[group, me_q], s3s, s3r.at[b], (z * NQ + q, t))
+        for p in range(low, high):
+            ret[p, me_q] = res[p, 0]
+
+    flying = []
+    for b in range(len(PASSES)):
+        flying.append((b, *begin(b)))
+        if len(flying) > FLIGHT:
+            finish(*flying.pop(0))
+    for item in flying:
+        finish(*item)
 
     wait_for("weights", recvm.at[pl.ds(1, NZ - 1)], smr)
-    row = iota((8 * BATCH, PER * picks), 0) // 8
-    column = iota((8 * BATCH, PER * picks), 1)
-    own = row == column // picks * PIECE + lax.rem(column // 2, PIECE)
-    weigh = []
-    for b in range(2):
-        meta = recvm[b * BATCH : (b + 1) * BATCH].reshape(8 * BATCH, 128)
+    for b, (low, high) in enumerate(PASSES):
+        count = high - low
+        meta = recvm[low:high].reshape(8 * count, 128)
         meta_hi = meta.astype(BF16)
         meta_lo = (meta - meta_hi.astype(F32)).astype(BF16)
+        own = iota((8 * count, picks * count), 0) // 8 == iota((8 * count, picks * count), 1) // picks
+        weigh = []
         for half_meta in (meta_hi, meta_lo):
-            spread = nt_dot(half_meta, expand)
-            weigh.append(jnp.where(own, jnp.concatenate([spread] * PER, axis=1), 0.0).astype(BF16))
-
-    for b in range(2):
-        wait_for("hop3", ret.at[b, :, pl.ds(1, NQ - 1)], s3r.at[b])
-        results = ret[b].astype(F32).reshape(PER * picks, half).astype(BF16)
-        summed = jnp.dot(weigh[2 * b], results, preferred_element_type=F32)
-        summed += jnp.dot(weigh[2 * b + 1], results, preferred_element_type=F32)
-        for k in range(BATCH):
-            p = b * BATCH + k
-            comb[p] = summed[8 * k : 8 * k + 8].astype(BF16)
-        for k in range(BATCH):
-            p = b * BATCH + k
+            spread = jnp.concatenate([nt_dot(half_meta, expand)] * count, axis=1)
+            weigh.append(jnp.where(own, spread, 0.0).astype(BF16))
+        wait_for("hop3", ret.at[pl.ds(low, count), others_q], s3r.at[b])
+        results = ret[low:high].astype(F32).reshape(count * picks, half).astype(BF16)
+        summed = jnp.dot(weigh[0], results, preferred_element_type=F32)
+        summed += jnp.dot(weigh[1], results, preferred_element_type=F32)
+        for p in range(low, high):
+            comb[p] = summed[8 * (p - low) : 8 * (p - low) + 8].astype(BF16)
+        for p in range(low, high):
             if p:
                 along_z(comb.at[p], back.at[z], s4s, s4r, -ORDER[p])
     back[z] = comb[0]
@@ -397,7 +402,7 @@
     others = pl.ds(1, NZ - 1)
     for region, sem in (
         (sendc.at[others], scs), (send1.at[others], s1s), (sendm.at[others], sms), (comb.at[others], s4s),
-        (send2.at[:, pl.ds(1, NQ - 1)], s2s), (part, ps), (res.at[:, :, pl.ds(1, NQ - 1)], s3s),
+        (send2.at[:, others_q], s2s), (part, ps), (res.at[:, others_q], s3s),
     ):
         wait_for("sent", region, sem)
 
@@ -410,10 +415,9 @@
     small = (partial, tok, norm, rg, rex, routes)
     by_half = pltpu.VMEM((2, seqs, half), BF16)
     by_z = pltpu.VMEM((NZ, 8, half), BF16)
-    pieces = NZ // PIECE
-    in_q = pltpu.VMEM((pieces, NQ, 2 * PIECE, half), BF16)
-    out_q = pltpu.VMEM((2, PER, NQ, 2 * PIECE, half), BF16)
-    parts = pltpu.VMEM((2, 2, 2 * BATCH * NQ, 2 * fh), BF16)
+    by_q = pltpu.VMEM((NZ, NQ, 2, half), BF16)
+    parts = pltpu.VMEM((2, 2 * NZ * NQ, 2 * fh), BF16)
+    passes = len(PASSES)
     return pl.pallas_call(
         exchange_kernel,
         out_shape=jax.ShapeDtypeStruct((seqs, half), BF16),
@@ -433,21 +437,21 @@
             by_z,
             pltpu.VMEM((NZ, 8, 128), F32),
             pltpu.VMEM((NZ, 8, 128), F32),
-            in_q,
-            in_q,
+            by_q,
+            by_q,
             parts,
             parts,
-            out_q,
-            out_q,
+            by_q,
+            by_q,
             by_z,
             by_z,
             dma((len(small),)),
             dma((3,)), dma((3,)), dma((3,)),
             dma((1,)), dma((1,)),
-            dma, dma((pieces,)), dma, dma((pieces,)), dma, dma,
-            dma, dma((2,)),
-            dma, dma((2, 2)),
-            dma, dma((2,)),
+            dma, dma((NZ,)), dma, dma((NZ,)), dma, dma,
+            dma, dma((passes,)),
+            dma, dma((passes, 2)),
+            dma, dma((passes,)),
             dma, dma,
         ],
         compiler_params=pltpu.CompilerParams(

time: 48.5 us -> 47 us (0.969)
  Pallas kernels: 45.7 us -> 44.5 us
    pallas_call x1, Pallas kernels: 38.2 us -> 36.9 us  [exchange(): pl.pallas_call(exchange_kernel, out_shape=jax.ShapeDtypeStruct((seqs, hal...]
where the time goes in v5:
time: 47 us; the launch traced here: 46.6 us
  Pallas kernels  44.5 us (95%)
  local copies, waits for them, and re-layouts  1.47 us (3%)
  between operations  0.65 us (1%)
    pallas_call x1, Pallas kernels, exchange(): pl.pallas_call(exchange_kernel, out_shape=jax.ShapeDtypeStruct((seqs, hal...  36.9 us
    pallas_call x1, Pallas kernels, front(): pl.pallas_call(front_kernel, out_shape=(jax.ShapeDtypeStruct(tok.shape, F...  7.56 us
    unnamed x1, local copies, waits for them, and re-layouts  1.47 us

profile of v5, /device:TPU:1, one launch (start us, length us, event | category | flops | bytes accessed | tf_op | source)
XLA Modules:
  0.0 46.6 jit_solution(14697147016435766542)
XLA Ops:
  0.6 7.6 %shard_map.221 = (f32[32,2048]{1,0:T(8,128)}, f32[32,4,64,64]{3,2,1,0:T(8,128)}) custom-call(bf16[32,2048]{1,0:T(8,128)(2,1)} %tok_ref.3, bf16[2048]{0:T(1024)(128)(2,1)} %norm_ref.2, bf16[2048,256]{1,0:T(8,128)(2,1)} %wr_ref.1, bf16[2048,256]{1,0:T(8,128)(2,1)} %wk_ref.1, bf16[2048,256]{1,0:T(8,128)(2,1)} %wv_ref.1, bf16[64,2048]{1,0:T(8,128)(2,1)} %bitcast.4, ...), custom_call_target="tpu_custom_call" | custom-call | tf_op jit(solution)/shard_map/pallas_call | solution.py:161
  8.2 36.9 %shard_map.222 = bf16[32,1024]{1,0:T(8,128)(2,1)} custom-call(f32[32,2048]{1,0:T(8,128)} %get-tuple-element.4.partial_ref, bf16[32,2048]{1,0:T(8,128)(2,1)} %tok_ref.3, bf16[2048]{0:T(1024)(128)(2,1)} %norm_ref.3, bf16[16,2048]{1,0:T(8,128)(2,1)} %bitcast.6, bf16[2048,128]{1,0:T(8,128)(2,1)} %re_ref.1, s32[4,32]{1,0:T(4,128)} %bitcast.7, ...), custom_call_target="tpu_custom_call" | custom-call | tf_op jit(solution)/shard_map/pallas_call | solution.py:421
  45.1 1.5 %copy.25 = bf16[32,1024]{1,0:T(8,128)(2,1)} copy(bf16[32,1024]{1,0:T(8,128)(2,1)} %shard_map.222) | data formatting | bytes 131072

commit v6 on v5

--- a/solution.py
+++ b/solution.py
@@ -120,7 +120,7 @@
     right = jnp.concatenate([by_head(-unit_key * learn), by_head(key_mod)], axis=0).astype(BF16)
     reads = by_head(recept.astype(F32)).astype(BF16)
     pick = jnp.where(iota((seqs, pairs), 0) == lax.rem(iota((seqs, pairs), 1), seqs), 1.0, 0.0).astype(BF16)
-    spread = lax.dot_general(value, pick, (((0,), (0,)), ((), ())), preferred_element_type=F32)
+    spread = lax.dot_general(value, pick, (((0,), (0,)), ((), ())), preferred_element_type=F32).astype(BF16)
 
     lane = iota((hs, pairs), 1)
     tall[...] = jnp.zeros_like(tall)
@@ -132,7 +132,7 @@
                 own = lane == h * seqs + s
                 rows = slice(h * hs, (h + 1) * hs)
                 lhs[s - c * chunk, rows, :pairs] = jnp.where(own, found[rows], 0.0).astype(BF16)
-                lhs[s - c * chunk, rows, pairs:] = jnp.where(own, spread[rows], 0.0).astype(BF16)
+                lhs[s - c * chunk, rows, pairs:] = jnp.where(own, spread[rows], jnp.zeros((), BF16))
         for s in range(c * chunk, (c + 1) * chunk):
             update = jnp.dot(lhs[s - c * chunk], right, preferred_element_type=F32)
             for h in range(heads):

time: 47 us -> 46.8 us (level)
  no operation moved by 1% of the time
where the time goes in v6:
time: 46.8 us; the launch traced here: 46.6 us
  Pallas kernels  44.5 us (95%)
  local copies, waits for them, and re-layouts  1.47 us (3%)
  between operations  0.65 us (1%)
    pallas_call x1, Pallas kernels, exchange(): pl.pallas_call(exchange_kernel, out_shape=jax.ShapeDtypeStruct((seqs, hal...  36.9 us
    pallas_call x1, Pallas kernels, front(): pl.pallas_call(front_kernel, out_shape=(jax.ShapeDtypeStruct(tok.shape, F...  7.56 us
    unnamed x1, local copies, waits for them, and re-layouts  1.47 us

profile of v6, /device:TPU:1, one launch (start us, length us, event | category | flops | bytes accessed | tf_op | source)
XLA Modules:
  0.0 46.6 jit_solution(6011714962743665116)
XLA Ops:
  0.6 7.6 %shard_map.221 = (f32[32,2048]{1,0:T(8,128)}, f32[32,4,64,64]{3,2,1,0:T(8,128)}) custom-call(bf16[32,2048]{1,0:T(8,128)(2,1)} %tok_ref.3, bf16[2048]{0:T(1024)(128)(2,1)} %norm_ref.2, bf16[2048,256]{1,0:T(8,128)(2,1)} %wr_ref.1, bf16[2048,256]{1,0:T(8,128)(2,1)} %wk_ref.1, bf16[2048,256]{1,0:T(8,128)(2,1)} %wv_ref.1, bf16[64,2048]{1,0:T(8,128)(2,1)} %bitcast.4, ...), custom_call_target="tpu_custom_call" | custom-call | tf_op jit(solution)/shard_map/pallas_call | solution.py:161
  8.2 36.9 %shard_map.222 = bf16[32,1024]{1,0:T(8,128)(2,1)} custom-call(f32[32,2048]{1,0:T(8,128)} %get-tuple-element.4.partial_ref, bf16[32,2048]{1,0:T(8,128)(2,1)} %tok_ref.3, bf16[2048]{0:T(1024)(128)(2,1)} %norm_ref.3, bf16[16,2048]{1,0:T(8,128)(2,1)} %bitcast.6, bf16[2048,128]{1,0:T(8,128)(2,1)} %re_ref.1, s32[4,32]{1,0:T(4,128)} %bitcast.7, ...), custom_call_target="tpu_custom_call" | custom-call | tf_op jit(solution)/shard_map/pallas_call | solution.py:421
  45.2 1.5 %copy.25 = bf16[32,1024]{1,0:T(8,128)(2,1)} copy(bf16[32,1024]{1,0:T(8,128)(2,1)} %shard_map.222) | data formatting | bytes 131072
